TPU v7x, 32 devices: a whole 2x2x4 slice. The times are simulated.
32 devices in a mesh: grp: 2 (over y), ep: 16 (over z, x, core), tp: 1.
Axes of the slice: x: 2, y: 2, z: 4, core: 2. Of those that a mesh axis runs over, the one named last changes fastest.
Arguments:
- tokens: bfloat16 [3072, 2048], P(('grp', 'ep')), parts along dimension 0, may hold values from -6 to 6
- prior_state: float32 [2, 3072, 4096], P(None, ('grp', 'ep'), 'tp'), parts along dimension 1, may hold values from -6 to 6
- mix_gain: float32 [2048], replicated, may hold values from 0.1 to 1.9
- in_weight: bfloat16 [2048, 1024], P(None, 'tp'), may hold values from -0.125 to 0.125
- decay_rate: float32 [64, 64], P('tp'), may hold values from 0.2 to 20
- frequency: float32 [64, 64], P('tp'), may hold values from 0 to 12
- log_step: float32 [64], P('tp'), may hold values from -4.6 to 0
- input_map: float32 [2, 64, 64, 16], P(None, 'tp'), may hold values from -6 to 6
- output_map: float32 [2, 64, 16, 64], P(None, 'tp'), may hold values from -0.5 to 0.5
- skip_gain: float32 [1024], P('tp'), may hold values from -4 to 4
- out_weight: bfloat16 [1024, 2048], P('tp'), may hold values from -0.1875 to 0.1875
- channel_gain: float32 [2048], replicated, may hold values from 0.1 to 1.9
- expert_gate: bfloat16 [16, 2048, 512], P('ep', None, 'tp'), may hold values from -0.125 to 0.125
- expert_up: bfloat16 [16, 2048, 512], P('ep', None, 'tp'), may hold values from -0.125 to 0.125
- expert_down: bfloat16 [16, 512, 2048], P('ep', 'tp'), may hold values from -0.25 to 0.25
- shared_gate: bfloat16 [2048, 512], P(None, 'tp'), may hold values from -0.125 to 0.125
- shared_up: bfloat16 [2048, 512], P(None, 'tp'), may hold values from -0.125 to 0.125
- shared_down: bfloat16 [512, 2048], P('tp'), may hold values from -0.25 to 0.25
- routes: int32 [3072, 6], P(('grp', 'ep')), parts along dimension 0, may hold values from 0 to 15, all different within a row; in each aligned block of 96 rows (0 to 95, 96 to 191, ...) at most 54 rows name the same one
- route_weights: float32 [3072, 6], P(('grp', 'ep')), parts along dimension 0, may hold values from 0.05 to 0.8
Outputs:
- layer_out: bfloat16 [3072, 2048], P(('grp', 'ep'), 'tp'), parts along dimension 0
- new_state: float32 [2, 3072, 4096], P(None, ('grp', 'ep'), 'tp'), parts along dimension 1
There are 2 independent parts, one for each index of `grp`. A program takes and returns all parts, laid end to end along the dimension named above; an argument that names none is the same for every part. Nothing has to cross between parts.
Inputs may be any that keep to these rules, and one draw needn't show every extreme that they name: `routes`: each row names 6 different experts; among the rows of one index of ep no expert is named by more than 54 rows.
All inputs are finite; a program needn't handle non-finite values.
Results may differ from a plain program's by a relative error of at most 0.017.
Values may be sent and summed in bfloat16 or wider, within the bound.
A program may use at most 128 MiB of HBM per device.

v0:
```python
import jax
import jax.numpy as jnp
from jax import lax
from jax.sharding import PartitionSpec as P

norm_eps = 1e-06
highest = lax.Precision.HIGHEST


def root_scale(activations, scale_gain):
    values = activations.astype(jnp.float32)
    factor = lax.rsqrt(jnp.mean(values * values, axis=-1, keepdims=True) + norm_eps)
    return (values * factor * scale_gain).astype(jnp.bfloat16)


def state_update(
    drive_rows, prior_state, decay_rate, frequency, log_step, input_map, output_map, skip_gain
):
    sequences = drive_rows.shape[0]
    groups = decay_rate.shape[0]
    driven = drive_rows.astype(jnp.float32).reshape(sequences, groups, -1)
    step_size = jnp.exp(log_step)[:, None]
    real_rate = -decay_rate
    magnitude = jnp.exp(real_rate * step_size)
    turn_real = magnitude * jnp.cos(frequency * step_size)
    turn_imag = magnitude * jnp.sin(frequency * step_size)
    denominator = real_rate * real_rate + frequency * frequency
    hold_real = ((turn_real - 1.0) * real_rate + turn_imag * frequency) / denominator
    hold_imag = (turn_imag * real_rate - (turn_real - 1.0) * frequency) / denominator
    push_real = jnp.einsum("sgh,gph->sgp", driven, input_map[0], precision=highest)
    push_imag = jnp.einsum("sgh,gph->sgp", driven, input_map[1], precision=highest)
    enter_real = push_real * hold_real - push_imag * hold_imag
    enter_imag = push_real * hold_imag + push_imag * hold_real
    old_real = prior_state[0].reshape(sequences, groups, -1)
    old_imag = prior_state[1].reshape(sequences, groups, -1)
    fresh_real = turn_real * old_real - turn_imag * old_imag + enter_real
    fresh_imag = turn_real * old_imag + turn_imag * old_real + enter_imag
    readout = jnp.einsum("ghp,sgp->sgh", output_map[0], fresh_real, precision=highest)
    readout = readout - jnp.einsum("ghp,sgp->sgh", output_map[1], fresh_imag, precision=highest)
    readout = readout.reshape(sequences, -1) + skip_gain * drive_rows.astype(jnp.float32)
    fresh = jnp.stack([fresh_real.reshape(sequences, -1), fresh_imag.reshape(sequences, -1)])
    return (readout, fresh)


def body(
    tokens,
    prior_state,
    mix_gain,
    in_weight,
    decay_rate,
    frequency,
    log_step,
    input_map,
    output_map,
    skip_gain,
    out_weight,
    channel_gain,
    expert_gate,
    expert_up,
    expert_down,
    shared_gate,
    shared_up,
    shared_down,
    routes,
    route_weights,
):
    normed = root_scale(tokens, mix_gain)
    drive_rows = jnp.dot(normed, in_weight, preferred_element_type=jnp.float32).astype(jnp.bfloat16)
    readout, new_state = state_update(
        drive_rows, prior_state, decay_rate, frequency, log_step, input_map, output_map, skip_gain
    )
    activated = jax.nn.gelu(readout).astype(jnp.bfloat16)
    partial_value = jnp.dot(activated, out_weight, preferred_element_type=jnp.float32)
    mixer_out = lax.psum(partial_value.astype(jnp.bfloat16), "tp").astype(jnp.float32)
    middle = (tokens.astype(jnp.float32) + mixer_out).astype(jnp.bfloat16)
    second_normed = root_scale(middle, channel_gain)
    shared_gval = jnp.dot(second_normed, shared_gate, preferred_element_type=jnp.float32)
    shared_uval = jnp.dot(second_normed, shared_up, preferred_element_type=jnp.float32)
    shared_hidden = (jax.nn.silu(shared_gval) * shared_uval).astype(jnp.bfloat16)
    shared_piece = jnp.dot(shared_hidden, shared_down, preferred_element_type=jnp.float32)
    shared_out = lax.psum_scatter(
        shared_piece.astype(jnp.bfloat16), "tp", scatter_dimension=1, tiled=True
    ).astype(jnp.float32)
    experts = lax.axis_size("ep")
    seq_rows, top_count = routes.shape
    slot_cap = min(seq_rows, max(2, 3 * seq_rows * top_count // (2 * experts)))
    flat_routes = routes.reshape(-1)
    one_hot = (flat_routes[:, None] == jnp.arange(experts, dtype=jnp.int32)[None, :]).astype(
        jnp.int32
    )
    ranked = jnp.sum((jnp.cumsum(one_hot, axis=0) - one_hot) * one_hot, axis=1)
    slot_index = flat_routes * slot_cap + ranked
    placed = slot_index[:, None] == jnp.arange(experts * slot_cap, dtype=jnp.int32)[None, :]
    placed_rows = jnp.any(placed.reshape(seq_rows, top_count, experts * slot_cap), axis=1).astype(
        jnp.bfloat16
    )
    outgoing = lax.dot_general(
        placed_rows, second_normed, (((0,), (0,)), ((), ())), preferred_element_type=jnp.float32
    ).astype(jnp.bfloat16)
    outgoing = outgoing.reshape(experts, slot_cap, -1)
    half_cols = outgoing.shape[2] // lax.axis_size("tp")
    arrived = lax.all_to_all(outgoing, "ep", split_axis=0, concat_axis=0, tiled=True)
    sources, count_items, full_width = arrived.shape
    expert_rows = arrived.reshape(sources * count_items, full_width)
    gate_val = jnp.dot(expert_rows, expert_gate[0], preferred_element_type=jnp.float32)
    up_val = jnp.dot(expert_rows, expert_up[0], preferred_element_type=jnp.float32)
    hidden = (jax.nn.silu(gate_val) * up_val).astype(jnp.bfloat16)
    piece = jnp.dot(hidden, expert_down[0], preferred_element_type=jnp.float32)
    summed = lax.psum_scatter(
        piece.reshape(sources, count_items, full_width).astype(jnp.bfloat16),
        "tp",
        scatter_dimension=2,
        tiled=True,
    )
    returned = lax.all_to_all(summed, "ep", split_axis=0, concat_axis=0, tiled=True)
    flat_back = returned.reshape(experts * slot_cap, -1)
    picked = (
        jnp.take(flat_back, slot_index, axis=0).reshape(seq_rows, top_count, -1).astype(jnp.float32)
    )
    routed = jnp.einsum("sk,skd->sd", route_weights, picked)
    own_middle = lax.dynamic_slice_in_dim(middle, lax.axis_index("tp") * half_cols, half_cols, 1)
    layer_out = (own_middle.astype(jnp.float32) + routed + shared_out).astype(jnp.bfloat16)
    return (layer_out, new_state)


def solution(mesh):
    in_specs = (
        P(("grp", "ep"), None),
        P(None, ("grp", "ep"), "tp"),
        P(),
        P(None, "tp"),
        P("tp", None),
        P("tp", None),
        P("tp"),
        P(None, "tp", None, None),
        P(None, "tp", None, None),
        P("tp"),
        P("tp", None),
        P(),
        P("ep", None, "tp"),
        P("ep", None, "tp"),
        P("ep", "tp", None),
        P(None, "tp"),
        P(None, "tp"),
        P("tp", None),
        P(("grp", "ep"), None),
        P(("grp", "ep"), None),
    )
    out_specs = (P(("grp", "ep"), "tp"), P(None, ("grp", "ep"), "tp"))
    return jax.shard_map(body, mesh=mesh, in_specs=in_specs, out_specs=out_specs, check_vma=False)
```

profile of v0, /device:TPU:15, one launch (start us, length us, event | category | flops | bytes accessed | tf_op | source)
XLA Modules:
  0.0 266.3 jit_solution(13506024707845342241)
XLA Ops:
  0.6 0.0 copy-start
  0.6 0.8 exp.14
  1.5 1.2 fusion.20
  2.6 0.8 copy.56
  3.4 0.1 reshape.118
  3.6 1.4 reduce-window.6
  5.0 0.2 slice_reduce_fusion
  5.3 0.1 bitcast_bitcast_fusion
  5.4 0.1 reduce_sum.33
  5.6 0.1 copy.59
  5.6 0.7 compare_and_fusion
  6.3 1.0 fusion.15
  7.3 3.2 %convolution_convert_fusion.4 = bf16[96,1024]{1,0:T(8,128)(2,1)S(1)} fusion(bf16[2048,1024]{1,0:T(8,128)(2,1)} %param.23, bf16[96,2048]{1,0:T(8,128)(2,1)} %param.20, f32[2048]{0:T(1024)} %param.22, f32[96]{0:T(128)S(1)} %add_rsqrt_fusion.1), kind=kOutput, calls=%fused_computation.30 | convolution fusion | flops 403537920 | bytes 4792704 | tf_op jit(solution)/shard_map/dot_general | solution.py:68
  10.5 0.2 copy.54
  10.7 3.8 %fusion.69 = (f32[1,96,4096]{2,1,0:T(8,128)}, f32[1,96,4096]{2,1,0:T(8,128)}) fusion(f32[2,96,4096]{2,1,0:T(8,128)} %param.21), kind=kLoop, calls=%fused_computation.104 | loop fusion | bytes 6291456 | tf_op jit(solution)/shard_map/slice | solution.py:34
  14.6 2.8 %copy.52 = f32[1,96,4096]{1,2,0:T(8,128)} copy(f32[1,96,4096]{2,1,0:T(8,128)} %get-tuple-element.6) | data formatting | bytes 3145728 | tf_op jit(solution)/shard_map/slice | solution.py:34
  17.3 2.9 %copy.53 = f32[1,96,4096]{1,2,0:T(8,128)} copy(f32[1,96,4096]{2,1,0:T(8,128)} %get-tuple-element.7) | data formatting | bytes 3145728 | tf_op jit(solution)/shard_map/slice | solution.py:35
  20.2 3.0 %fusion.28 = f32[64,96,64]{1,2,0:T(8,128)S(1)} fusion(bf16[96,64,16]{0,2,1:T(8,128)(2,1)S(1)} %bitcast.74, f32[2,64,64,16]{2,3,1,0:T(8,128)} %param.27), kind=kOutput, calls=%fused_computation.45 | convolution fusion | flops 75497472 | bytes 2293760 | tf_op jit(solution)/shard_map/sgh,gph->sgp/dot_general | solution.py:30
  23.2 0.2 cosine_multiply_fusion
  23.5 5.7 %bitcast_add_fusion = (f32[96,64,64]{0,2,1:T(8,128)S(1)}, f32[96,64,64]{0,2,1:T(8,128)S(1)}) fusion(f32[64,96,64]{1,2,0:T(8,128)S(1)} %fusion.28, f32[96,64,64]{0,2,1:T(8,128)S(1)} %bitcast.72, f32[96,64,64]{0,2,1:T(8,128)} %bitcast.73, f32[64,64]{1,0:T(8,128)S(1)} %get-tuple-element.10, f32[64,64]{1,0:T(8,128)S(1)} %get-tuple-element.9, ...), kind=kOutput, calls=%fused_computation.21 | convolution fusion | flops 81002496 | bytes 9175040 | tf_op jit(solution)/shard_map/sgh,gph->sgp/dot_general | solution.py:31
  29.2 1.9 fusion.24
  31.2 0.0 copy-start.14
  31.2 1.9 convolution_subtract_fusion
  33.1 0.9 copy.55
  34.1 3.3 %multiply_reduce_fusion = (f32[96]{0:T(128)S(1)}, f32[96,2048]{1,0:T(8,128)S(1)}) fusion(bf16[1024,2048]{1,0:T(8,128)(2,1)} %param.30, f32[96,1024]{1,0:T(8,128)} %copy.55, bf16[96,1024]{1,0:T(8,128)(2,1)S(1)} %convolution_convert_fusion.4, f32[1024]{0:T(1024)S(1)} %copy-done.14, bf16[96,2048]{1,0:T(8,128)(2,1)S(1)} %copy-done.6), kind=kOutput, calls=%fused_computation.38 | convolution fusion | flops 405405600 | bytes 5968256 | tf_op jit(solution)/shard_map/dot_general | solution.py:73
  37.4 2.9 %convolution_convert_fusion.1 = bf16[864,2048]{1,0:T(8,128)(2,1)} fusion(pred[96,864]{1,0:T(8,128)(4,1)S(1)} %copy-done.8, f32[96,2048]{1,0:T(8,128)S(1)} %get-tuple-element.13, f32[2048]{0:T(1024)S(1)} %copy-done.9, f32[96]{0:T(128)S(1)} %add_rsqrt_fusion), kind=kOutput, calls=%fused_computation.2 | convolution fusion | flops 342097920 | bytes 4416896 | tf_op jit(solution)/shard_map/dot_general | solution.py:97
  40.4 4.8 %reshape.121 = bf16[16,54,2048]{2,1,0:T(8,128)(2,1)} reshape(bf16[864,2048]{1,0:T(8,128)(2,1)} %convolution_convert_fusion.1) | data formatting | bytes 7077888 | tf_op jit(solution)/shard_map/reshape | solution.py:100
  45.1 87.6 %all_to_all.10 = bf16[16,54,2048]{2,1,0:T(8,128)(2,1)} all-to-all(bf16[16,54,2048]{2,1,0:T(8,128)(2,1)} %reshape.121), channel_id=1, replica_groups=mesh['grp'=2,'ep'=16,'tp'=1] {'ep'}, dimensions={0} | all-to-all | bytes 7077888 | tf_op jit(solution)/shard_map/all_to_all | solution.py:102
  132.7 4.8 %reshape.122 = bf16[864,2048]{1,0:T(8,128)(2,1)} reshape(bf16[16,54,2048]{2,1,0:T(8,128)(2,1)} %all_to_all.10) | data formatting | bytes 7077888 | tf_op jit(solution)/shard_map/reshape | solution.py:104
  137.5 4.8 %fusion.13 = f32[864,512]{1,0:T(8,128)S(1)} fusion(bf16[864,2048]{1,0:T(8,128)(2,1)} %reshape.122, bf16[1,2048,512]{2,1,0:T(8,128)(2,1)} %param.32), kind=kOutput, calls=%fused_computation.19 | convolution fusion | flops 1811939328 | bytes 7405568 | tf_op jit(solution)/shard_map/dot_general | solution.py:105
  142.3 3.1 %multiply_convert_fusion = bf16[864,512]{1,0:T(8,128)(2,1)} fusion(f32[864,512]{1,0:T(8,128)S(1)} %fusion.13, bf16[864,2048]{1,0:T(8,128)(2,1)S(1)} %copy-done.5, bf16[1,2048,512]{2,1,0:T(8,128)(2,1)S(1)} %copy-done.15), kind=kOutput, calls=%fused_computation.25 | convolution fusion | flops 1814593536 | bytes 8290304 | tf_op jit(solution)/shard_map/dot_general | solution.py:106
  145.4 2.2 dot_general.53
  147.6 5.1 %convolution_convert_fusion = bf16[16,54,2048]{2,1,0:T(8,128)(2,1)} fusion(bf16[16,54,512]{2,1,0:T(8,128)(2,1)} %dot_general.53, bf16[1,512,2048]{2,1,0:T(8,128)(2,1)S(1)} %copy-done), kind=kOutput, calls=%fused_computation.1 | convolution fusion | flops 1813708800 | bytes 6520832 | tf_op jit(solution)/shard_map/dot_general | solution.py:108
  152.7 5.3 %all-to-all-start.1 = ((bf16[16,54,2048]{2,1,0:T(8,128)(2,1)}), bf16[16,54,2048]{2,1,0:T(8,128)(2,1)}, u32[]{:S(2)}, u32[]{:S(2)}) async-start(bf16[16,54,2048]{2,1,0:T(8,128)(2,1)} %convolution_convert_fusion), calls=%async_computation.1 | async-start | bytes 7340032 | tf_op jit(solution)/shard_map/all_to_all | solution.py:115
  158.0 0.1 copy.61
  158.1 0.1 mul.256
  158.3 0.1 copy.64
  158.4 0.1 copy.60
  158.6 2.8 %copy.62 = f32[1,96,4096]{2,1,0:T(8,128)} copy(f32[1,96,4096]{1,2,0:T(8,128)} %bitcast.71) | data formatting | bytes 3145728 | tf_op jit(solution)/shard_map/stack;reshape | solution.py:41
  161.4 2.8 %copy.63 = f32[1,96,4096]{2,1,0:T(8,128)} copy(f32[1,96,4096]{1,2,0:T(8,128)} %bitcast.70) | data formatting | bytes 3145728 | tf_op jit(solution)/shard_map/stack;reshape | solution.py:41
  164.2 2.2 fusion.67
  166.4 3.3 %pad_maximum_fusion = f32[2,96,4096]{2,1,0:T(8,128)} fusion(f32[1,96,4096]{2,1,0:T(8,128)} %copy.63, f32[1,96,4096]{2,1,0:T(8,128)S(1)} %copy-done.4), kind=kLoop, calls=%fused_computation.3 | loop fusion | flops 786432 | bytes 6291456 | tf_op jit(solution)/shard_map/stack | solution.py:41
  169.8 69.5 %all-to-all-done.1 = bf16[16,54,2048]{2,1,0:T(8,128)(2,1)} async-done(((bf16[16,54,2048]{2,1,0:T(8,128)(2,1)}), bf16[16,54,2048]{2,1,0:T(8,128)(2,1)}, u32[]{:S(2)}, u32[]{:S(2)}) %all-to-all-start.1) | async-done | bytes 3538976 | tf_op jit(solution)/shard_map/all_to_all | solution.py:115
  239.2 4.7 %reshape.123 = bf16[864,2048]{1,0:T(8,128)(2,1)} reshape(bf16[16,54,2048]{2,1,0:T(8,128)(2,1)} %all-to-all-done.1) | data formatting | bytes 7077888 | tf_op jit(solution)/shard_map/reshape | solution.py:116
  244.0 9.3 %gather_fusion = bf16[576,2048]{1,0:T(8,128)(2,1)} fusion(bf16[864,2048]{1,0:T(8,128)(2,1)} %reshape.123, s32[1024]{0:T(1024)S(1)} %pad_clamp_fusion), kind=kCustom, calls=%fused_computation | custom fusion | bytes 4720896 | tf_op jit(solution)/shard_map/jit(_take)/gather | solution.py:118
  253.3 5.0 %gather.7 = bf16[96,6,2048]{2,1,0:T(8,128)(2,1)} reshape(bf16[576,2048]{1,0:T(8,128)(2,1)} %gather_fusion) | data formatting | bytes 4718592 | tf_op jit(solution)/shard_map/jit(_take)/gather | solution.py:118
  258.3 3.8 %fusion = f32[96,1,2048]{2,1,0:T(1,128)} fusion(bf16[96,6,1]{1,2,0:T(2,128)(2,1)S(1)} %copy.64, bf16[96,6,2048]{2,1,0:T(8,128)(2,1)} %gather.7, pred[96,6]{1,0:T(8,128)(4,1)S(1)} %copy.60), kind=kOutput, calls=%fused_computation.4 | convolution fusion | flops 3538944 | bytes 3147456 | tf_op jit(solution)/shard_map/sk,skd->sd/dot_general | solution.py:120
  262.1 4.2 %fusion.5 = bf16[96,2048]{1,0:T(8,128)(2,1)} fusion(bf16[512,2048]{1,0:T(8,128)(2,1)} %param.37, bf16[2048,512]{1,0:T(8,128)(2,1)} %param.36, f32[96,2048]{1,0:T(8,128)S(1)} %get-tuple-element.13, f32[96,1,2048]{2,1,0:T(1,128)} %fusion, f32[96,512]{1,0:T(8,128)S(1)} %fusion.67, f32[2048]{0:T(1024)S(1)} %copy-done.9, f32[96]{0:T(128)S(1)} %add_rsqrt_fusion), kind=kOutput, calls=%fused_computation.10 | convolution fusion | flops 404520960 | bytes 6365568 | tf_op jit(solution)/shard_map/dot_general | solution.py:80
  (39 shorter events, 0.2 us)
Async XLA Ops:
  0.6 147.0 %copy-start = (bf16[1,512,2048]{2,1,0:T(8,128)(2,1)S(1)}, bf16[1,512,2048]{2,1,0:T(8,128)(2,1)}, u32[]{:S(2)}) copy-start(bf16[1,512,2048]{2,1,0:T(8,128)(2,1)} %param.34) | copy-start | bytes 6291460
  20.2 3.0 %copy-start.11 = (f32[64,64]{1,0:T(8,128)S(1)}, f32[64,64]{1,0:T(8,128)}, u32[]{:S(2)}) copy-start(f32[64,64]{1,0:T(8,128)} %param.25) | copy-start | bytes 49156
  20.2 3.0 %copy-start.12 = (f32[64,64]{1,0:T(8,128)S(1)}, f32[64,64]{1,0:T(8,128)}, u32[]{:S(2)}) copy-start(f32[64,64]{1,0:T(8,128)} %param.24) | copy-start | bytes 49156
  20.2 3.3 %copy-start.3 = (f32[1,96,4096]{1,2,0:T(8,128)S(1)}, f32[1,96,4096]{1,2,0:T(8,128)}, u32[]{:S(2)}) copy-start(f32[1,96,4096]{1,2,0:T(8,128)} %copy.52) | copy-start | bytes 4718596
  23.5 5.8 %copy-start.7 = (f32[2,64,16,64]{3,2,1,0:T(8,128)S(1)}, f32[2,64,16,64]{3,2,1,0:T(8,128)}, u32[]{:S(2)}) copy-start(f32[2,64,16,64]{3,2,1,0:T(8,128)} %param.28) | copy-start | bytes 1572868
  29.2 3.9 %copy-start.1 = (f32[96,64,64]{0,2,1:T(8,128)}, f32[96,64,64]{0,2,1:T(8,128)S(1)}, u32[]{:S(2)}) copy-start(f32[96,64,64]{0,2,1:T(8,128)S(1)} %get-tuple-element.4) | copy-start | bytes 4718596
  29.2 3.9 %copy-start.2 = (f32[96,64,64]{0,2,1:T(8,128)}, f32[96,64,64]{0,2,1:T(8,128)S(1)}, u32[]{:S(2)}) copy-start(f32[96,64,64]{0,2,1:T(8,128)S(1)} %get-tuple-element.5) | copy-start | bytes 4718596
  31.2 2.9 %copy-start.6 = (bf16[96,2048]{1,0:T(8,128)(2,1)S(1)}, bf16[96,2048]{1,0:T(8,128)(2,1)}, u32[]{:S(2)}) copy-start(bf16[96,2048]{1,0:T(8,128)(2,1)} %param.20) | copy-start | bytes 1179652
  31.2 2.9 %copy-start.14 = (f32[1024]{0:T(1024)S(1)}, f32[1024]{0:T(1024)}, u32[]{:S(2)}) copy-start(f32[1024]{0:T(1024)} %param.29) | copy-start | bytes 12292
  34.1 3.4 %copy-start.8 = (pred[96,864]{1,0:T(8,128)(4,1)S(1)}, pred[96,864]{1,0:T(8,128)(4,1)}, u32[]{:S(2)}) copy-start(pred[96,864]{1,0:T(8,128)(4,1)} %fusion.15) | copy-start | bytes 248836
  34.1 3.4 %copy-start.9 = (f32[2048]{0:T(1024)S(1)}, f32[2048]{0:T(1024)}, u32[]{:S(2)}) copy-start(f32[2048]{0:T(1024)} %param.31) | copy-start | bytes 24580
  137.5 4.8 %copy-start.5 = (bf16[864,2048]{1,0:T(8,128)(2,1)S(1)}, bf16[864,2048]{1,0:T(8,128)(2,1)}, u32[]{:S(2)}) copy-start(bf16[864,2048]{1,0:T(8,128)(2,1)} %reshape.122) | copy-start | bytes 10616836
  137.5 4.8 %copy-start.15 = (bf16[1,2048,512]{2,1,0:T(8,128)(2,1)S(1)}, bf16[1,2048,512]{2,1,0:T(8,128)(2,1)}, u32[]{:S(2)}) copy-start(bf16[1,2048,512]{2,1,0:T(8,128)(2,1)} %param.33) | copy-start | bytes 6291460
  152.7 5.3 %copy-start.10 = (s32[96,6]{0,1:T(8,128)S(1)}, s32[96,6]{0,1:T(8,128)}, u32[]{:S(2)}) copy-start(s32[96,6]{0,1:T(8,128)} %param.38) | copy-start | bytes 6916
  152.7 5.5 %copy-start.13 = (f32[96,6]{0,1:T(8,128)S(1)}, f32[96,6]{0,1:T(8,128)}, u32[]{:S(2)}) copy-start(f32[96,6]{0,1:T(8,128)} %param.39) | copy-start | bytes 6916
  152.7 86.5 %all-to-all-start.1 = ((bf16[16,54,2048]{2,1,0:T(8,128)(2,1)}), bf16[16,54,2048]{2,1,0:T(8,128)(2,1)}, u32[]{:S(2)}, u32[]{:S(2)}) async-start(bf16[16,54,2048]{2,1,0:T(8,128)(2,1)} %convolution_convert_fusion), calls=%async_computation.1 | async-start | bytes 7340032 | tf_op jit(solution)/shard_map/all_to_all | solution.py:115
  164.2 2.3 copy-start.4
where the time goes:
time: 267 us; the launch traced here: 266 us
  blocking collectives  87.6 us (33%)
  waiting for transfers between devices  69.5 us (26%)
  local copies, waits for them, and re-layouts  49.7 us (19%)
  matrix products  45.3 us (17%)
  other arithmetic  8.05 us (3%)
  starting transfers between devices  5.27 us (2%)
    all_to_all x1, blocking collectives, body(): lax.all_to_all(outgoing, 'ep', split_axis=0, concat_axis=0, tiled=True)  87.6 us
    all_to_all x1, waiting for transfers between devices, body(): lax.all_to_all(summed, 'ep', split_axis=0, concat_axis=0, tiled=True)  69.5 us
    gather x2, local copies, waits for them, and re-layouts, body(): jnp.take(flat_back, slot_index, axis=0).reshape(seq_rows, top_count, -1)  14.3 us
    slice x2, local copies, waits for them, and re-layouts, state_update(): old_real = prior_state[0].reshape(sequences, groups, -1)  6.63 us
    dot_general x1, matrix products, state_update(): jnp.einsum('sgh,gph->sgp', driven, input_map[1], precision=highest)  5.71 us
    another operation x2, local copies, waits for them, and re-layouts, state_update(): jnp.stack([fresh_real.reshape(sequences, -1), fresh_imag.reshape(sequence...  5.62 us
  transfers between devices with their start and end apart: 1, of which 1 were waited for; matrix products, arithmetic and copies ran while one was open for 4% of the time, Pallas kernels for 0%

commit v1 on v0

--- a/solution.py
+++ b/solution.py
@@ -42,6 +42,61 @@
     return (readout, fresh)
 
 
+def exchanged_experts(second_normed, routes, route_weights, expert_gate, expert_up, expert_down):
+    experts = lax.axis_size("ep")
+    seq_rows, top_count = routes.shape
+    slot_cap = min(seq_rows, max(2, 3 * seq_rows * top_count // (2 * experts)))
+    flat_routes = routes.reshape(-1)
+    one_hot = (flat_routes[:, None] == jnp.arange(experts, dtype=jnp.int32)[None, :]).astype(
+        jnp.int32
+    )
+    ranked = jnp.sum((jnp.cumsum(one_hot, axis=0) - one_hot) * one_hot, axis=1)
+    slot_index = flat_routes * slot_cap + ranked
+    placed = slot_index[:, None] == jnp.arange(experts * slot_cap, dtype=jnp.int32)[None, :]
+    placed_rows = jnp.any(placed.reshape(seq_rows, top_count, experts * slot_cap), axis=1).astype(
+        jnp.bfloat16
+    )
+    outgoing = lax.dot_general(
+        placed_rows, second_normed, (((0,), (0,)), ((), ())), preferred_element_type=jnp.float32
+    ).astype(jnp.bfloat16)
+    outgoing = outgoing.reshape(experts, slot_cap, -1)
+    arrived = lax.all_to_all(outgoing, "ep", split_axis=0, concat_axis=0, tiled=True)
+    sources, count_items, full_width = arrived.shape
+    expert_rows = arrived.reshape(sources * count_items, full_width)
+    gate_val = jnp.dot(expert_rows, expert_gate[0], preferred_element_type=jnp.float32)
+    up_val = jnp.dot(expert_rows, expert_up[0], preferred_element_type=jnp.float32)
+    hidden = (jax.nn.silu(gate_val) * up_val).astype(jnp.bfloat16)
+    piece = jnp.dot(hidden, expert_down[0], preferred_element_type=jnp.float32)
+    summed = lax.psum_scatter(
+        piece.reshape(sources, count_items, full_width).astype(jnp.bfloat16),
+        "tp",
+        scatter_dimension=2,
+        tiled=True,
+    )
+    returned = lax.all_to_all(summed, "ep", split_axis=0, concat_axis=0, tiled=True)
+    flat_back = returned.reshape(experts * slot_cap, -1)
+    picked = (
+        jnp.take(flat_back, slot_index, axis=0).reshape(seq_rows, top_count, -1).astype(jnp.float32)
+    )
+    routed = jnp.einsum("sk,skd->sd", route_weights, picked)
+    return routed
+
+
+def gathered_experts(second_normed, routes, route_weights, expert_gate, expert_up, expert_down):
+    all_routes = lax.all_gather(routes, "ep", axis=0, tiled=True)
+    all_weights = lax.all_gather(route_weights, "ep", axis=0, tiled=True)
+    here = all_routes == lax.axis_index("ep")
+    weight = jnp.sum(jnp.where(here, all_weights, 0.0), axis=1)
+    rows = lax.all_gather(second_normed, "ep", axis=0, tiled=True)
+    gate_val = jnp.dot(rows, expert_gate[0], preferred_element_type=jnp.float32)
+    up_val = jnp.dot(rows, expert_up[0], preferred_element_type=jnp.float32)
+    hidden = (jax.nn.silu(gate_val) * up_val).astype(jnp.bfloat16)
+    piece = jnp.dot(hidden, expert_down[0], preferred_element_type=jnp.float32)
+    summed = lax.psum_scatter(piece.astype(jnp.bfloat16), "tp", scatter_dimension=1, tiled=True)
+    weighted = (weight[:, None] * summed.astype(jnp.float32)).astype(jnp.bfloat16)
+    return lax.psum_scatter(weighted, "ep", scatter_dimension=0, tiled=True).astype(jnp.float32)
+
+
 def body(
     tokens,
     prior_state,
@@ -82,42 +137,15 @@
         shared_piece.astype(jnp.bfloat16), "tp", scatter_dimension=1, tiled=True
     ).astype(jnp.float32)
     experts = lax.axis_size("ep")
-    seq_rows, top_count = routes.shape
-    slot_cap = min(seq_rows, max(2, 3 * seq_rows * top_count // (2 * experts)))
-    flat_routes = routes.reshape(-1)
-    one_hot = (flat_routes[:, None] == jnp.arange(experts, dtype=jnp.int32)[None, :]).astype(
-        jnp.int32
-    )
-    ranked = jnp.sum((jnp.cumsum(one_hot, axis=0) - one_hot) * one_hot, axis=1)
-    slot_index = flat_routes * slot_cap + ranked
-    placed = slot_index[:, None] == jnp.arange(experts * slot_cap, dtype=jnp.int32)[None, :]
-    placed_rows = jnp.any(placed.reshape(seq_rows, top_count, experts * slot_cap), axis=1).astype(
-        jnp.bfloat16
-    )
-    outgoing = lax.dot_general(
-        placed_rows, second_normed, (((0,), (0,)), ((), ())), preferred_element_type=jnp.float32
-    ).astype(jnp.bfloat16)
-    outgoing = outgoing.reshape(experts, slot_cap, -1)
-    half_cols = outgoing.shape[2] // lax.axis_size("tp")
-    arrived = lax.all_to_all(outgoing, "ep", split_axis=0, concat_axis=0, tiled=True)
-    sources, count_items, full_width = arrived.shape
-    expert_rows = arrived.reshape(sources * count_items, full_width)
-    gate_val = jnp.dot(expert_rows, expert_gate[0], preferred_element_type=jnp.float32)
-    up_val = jnp.dot(expert_rows, expert_up[0], preferred_element_type=jnp.float32)
-    hidden = (jax.nn.silu(gate_val) * up_val).astype(jnp.bfloat16)
-    piece = jnp.dot(hidden, expert_down[0], preferred_element_type=jnp.float32)
-    summed = lax.psum_scatter(
-        piece.reshape(sources, count_items, full_width).astype(jnp.bfloat16),
-        "tp",
-        scatter_dimension=2,
-        tiled=True,
-    )
-    returned = lax.all_to_all(summed, "ep", split_axis=0, concat_axis=0, tiled=True)
-    flat_back = returned.reshape(experts * slot_cap, -1)
-    picked = (
-        jnp.take(flat_back, slot_index, axis=0).reshape(seq_rows, top_count, -1).astype(jnp.float32)
-    )
-    routed = jnp.einsum("sk,skd->sd", route_weights, picked)
+    half_cols = second_normed.shape[1] // lax.axis_size("tp")
+    if experts <= 16:
+        routed = gathered_experts(
+            second_normed, routes, route_weights, expert_gate, expert_up, expert_down
+        )
+    else:
+        routed = exchanged_experts(
+            second_normed, routes, route_weights, expert_gate, expert_up, expert_down
+        )
     own_middle = lax.dynamic_slice_in_dim(middle, lax.axis_index("tp") * half_cols, half_cols, 1)
     layer_out = (own_middle.astype(jnp.float32) + routed + shared_out).astype(jnp.bfloat16)
     return (layer_out, new_state)

time: 267 us -> 220 us (0.82)
  the two profiles are of different devices: /device:TPU:15 before, /device:TPU:0 now
where the time goes in v1:
time: 220 us
  waiting for transfers between devices  94.8 us (43%)
  matrix products  45.6 us (21%)
  blocking collectives  42 us (19%)
  local copies, waits for them, and re-layouts  17.2 us (8%)
  between operations  14.2 us (6%)
  other arithmetic  5.75 us (3%)
    reduce_scatter x1, waiting for transfers between devices, gathered_experts(): lax.psum_scatter(weighted, 'ep', scatter_dimension=0, tiled=True)  72.4 us
    all_gather x1, blocking collectives, gathered_experts(): all_routes = lax.all_gather(routes, 'ep', axis=0, tiled=True)  23.8 us
    all_gather x1, waiting for transfers between devices, gathered_experts(): rows = lax.all_gather(second_normed, 'ep', axis=0, tiled=True)  22.4 us
    all_gather x1, blocking collectives, gathered_experts(): all_weights = lax.all_gather(route_weights, 'ep', axis=0, tiled=True)  18.2 us
    dot_general x1, matrix products, gathered_experts(): piece = jnp.dot(hidden, expert_down[0], preferred_element_type=jnp.float32)  11.8 us
    dot_general x1, matrix products, gathered_experts(): gate_val = jnp.dot(rows, expert_gate[0], preferred_element_type=jnp.float32)  8.51 us
    slice x2, local copies, waits for them, and re-layouts, state_update(): old_real = prior_state[0].reshape(sequences, groups, -1)  6.61 us
    another operation x2, local copies, waits for them, and re-layouts, state_update(): jnp.stack([fresh_real.reshape(sequences, -1), fresh_imag.reshape(sequence...  5.71 us
  transfers between devices with their start and end apart: 2, of which 2 were waited for; matrix products, arithmetic and copies ran while one was open for 5% of the time, Pallas kernels for 0%

profile of v1, /device:TPU:0, one launch (start us, length us, event | category | flops | bytes accessed | tf_op | source)
XLA Modules:
  0.0 219.6 jit_solution(10515037456347401280)
XLA Ops:
  7.2 0.0 copy-start
  7.2 0.0 all-gather.4.cloned.1.call-start
  7.2 0.8 exp.14
  8.0 1.2 fusion.13
  9.2 3.2 %convolution_convert_fusion.3 = bf16[96,1024]{1,0:T(8,128)(2,1)S(1)} fusion(bf16[2048,1024]{1,0:T(8,128)(2,1)} %param.23, bf16[96,2048]{1,0:T(8,128)(2,1)} %param.20, f32[2048]{0:T(1024)} %param.22, f32[96]{0:T(128)S(1)} %add_rsqrt_fusion.1), kind=kOutput, calls=%fused_computation.23 | convolution fusion | flops 403537920 | bytes 4792704 | tf_op jit(solution)/shard_map/dot_general | solution.py:123
  12.4 0.2 copy.37
  12.6 3.8 %fusion.58 = (f32[1,96,4096]{2,1,0:T(8,128)}, f32[1,96,4096]{2,1,0:T(8,128)}) fusion(f32[2,96,4096]{2,1,0:T(8,128)} %param.21), kind=kLoop, calls=%fused_computation.79 | loop fusion | bytes 6291456 | tf_op jit(solution)/shard_map/slice | solution.py:34
  16.4 2.8 %copy.35 = f32[1,96,4096]{1,2,0:T(8,128)} copy(f32[1,96,4096]{2,1,0:T(8,128)} %get-tuple-element.4) | data formatting | bytes 3145728 | tf_op jit(solution)/shard_map/slice | solution.py:34
  19.2 2.8 %copy.36 = f32[1,96,4096]{1,2,0:T(8,128)} copy(f32[1,96,4096]{2,1,0:T(8,128)} %get-tuple-element.5) | data formatting | bytes 3145728 | tf_op jit(solution)/shard_map/slice | solution.py:35
  22.0 3.0 %fusion.23 = f32[64,96,64]{1,2,0:T(8,128)S(1)} fusion(bf16[96,64,16]{0,2,1:T(8,128)(2,1)S(1)} %bitcast.56, f32[2,64,64,16]{2,3,1,0:T(8,128)} %param.27), kind=kOutput, calls=%fused_computation.37 | convolution fusion | flops 75497472 | bytes 2293760 | tf_op jit(solution)/shard_map/sgh,gph->sgp/dot_general | solution.py:30
  25.1 0.0 copy-done.8
  25.1 0.0 copy-done.9
  25.1 0.2 cosine_multiply_fusion
  25.3 0.0 copy-done.3
  25.3 0.0 copy-start.7
  25.3 5.7 %bitcast_add_fusion = (f32[96,64,64]{0,2,1:T(8,128)S(1)}, f32[96,64,64]{0,2,1:T(8,128)S(1)}) fusion(f32[64,96,64]{1,2,0:T(8,128)S(1)} %fusion.23, f32[96,64,64]{0,2,1:T(8,128)S(1)} %bitcast.54, f32[96,64,64]{0,2,1:T(8,128)} %bitcast.55, f32[64,64]{1,0:T(8,128)S(1)} %get-tuple-element.8, f32[64,64]{1,0:T(8,128)S(1)} %get-tuple-element.7, ...), kind=kOutput, calls=%fused_computation.18 | convolution fusion | flops 81002496 | bytes 9175040 | tf_op jit(solution)/shard_map/sgh,gph->sgp/dot_general | solution.py:31
  31.0 0.0 copy-start.1
  31.0 0.0 copy-start.2
  31.1 0.0 copy-done.7
  31.1 1.9 fusion.19
  33.0 0.0 copy-start.13
  33.0 1.9 convolution_subtract_fusion
  34.9 0.0 copy-done.1
  34.9 0.0 copy-done.2
  34.9 0.9 copy.38
  35.9 0.0 copy-done.6
  35.9 0.0 copy-done.13
  35.9 0.0 copy-start.12
  35.9 3.3 %multiply_reduce_fusion = (f32[96]{0:T(128)S(1)}, f32[96,2048]{1,0:T(8,128)S(1)}) fusion(bf16[1024,2048]{1,0:T(8,128)(2,1)} %param.30, f32[96,1024]{1,0:T(8,128)} %copy.38, bf16[96,1024]{1,0:T(8,128)(2,1)S(1)} %convolution_convert_fusion.3, f32[1024]{0:T(1024)S(1)} %copy-done.13, bf16[96,2048]{1,0:T(8,128)(2,1)S(1)} %copy-done.6), kind=kOutput, calls=%fused_computation.30 | convolution fusion | flops 405405600 | bytes 5968256 | tf_op jit(solution)/shard_map/dot_general | solution.py:128
  39.2 0.0 copy-done.10
  39.2 0.9 multiply_convert_fusion.1
  40.1 0.0 all-gather.4.cloned.1.call-update
  40.2 0.0 reduce-scatter.2.cloned.1.call-start
  40.2 0.0 copy-done.11
  40.2 23.8 %all-gather = s32[16,96,6]{1,2,0:T(8,128)S(1)} all-gather(s32[1,96,6]{1,2,0:T(8,128)S(1)} %bitcast.59), channel_id=1, replica_groups=mesh['grp'=2,'ep'=16,'tp'=1] {'ep'}, dimensions={0}, use_global_device_ids=true | all-gather | bytes 39168 | tf_op jit(solution)/shard_map/all_gather | solution.py:86
  64.0 0.0 copy-done.12
  64.0 18.2 %all-gather.1 = f32[16,96,6]{1,2,0:T(8,128)S(1)} all-gather(f32[1,96,6]{1,2,0:T(8,128)S(1)} %bitcast.60), channel_id=1, replica_groups=mesh['grp'=2,'ep'=16,'tp'=1] {'ep'}, dimensions={0}, use_global_device_ids=true | all-gather | bytes 39168 | tf_op jit(solution)/shard_map/all_gather | solution.py:87
  82.2 0.1 reshape.45
  82.3 22.4 %all-gather.4.cloned.1.call-done = bf16[1536,2048]{1,0:T(8,128)(2,1)} async-done(((bf16[96,2048]{1,0:T(8,128)(2,1)}), bf16[1536,2048]{1,0:T(8,128)(2,1)}) %all-gather.4.cloned.1.call-update) | async-done | bytes 6291472 | tf_op jit(solution)/shard_map/all_gather | solution.py:90
  104.7 8.5 %fusion.10 = f32[1536,512]{1,0:T(8,128)} fusion(bf16[1536,2048]{1,0:T(8,128)(2,1)} %all-gather.4.cloned.1.call-done, bf16[1,2048,512]{2,1,0:T(8,128)(2,1)} %param.32), kind=kOutput, calls=%fused_computation.16 | convolution fusion | flops 3221225472 | bytes 11534336 | tf_op jit(solution)/shard_map/dot_general | solution.py:91
  113.2 11.8 %multiply_convert_fusion = bf16[1536,2048]{1,0:T(8,128)(2,1)} fusion(f32[1536]{0:T(1024)S(1)} %reshape.45, bf16[1,512,2048]{2,1,0:T(8,128)(2,1)S(1)} %copy-done, bf16[1536,2048]{1,0:T(8,128)(2,1)} %all-gather.4.cloned.1.call-done, f32[1536,512]{1,0:T(8,128)} %fusion.10, bf16[1,2048,512]{2,1,0:T(8,128)(2,1)} %param.33), kind=kOutput, calls=%fused_computation | convolution fusion | flops 6459752448 | bytes 19929088 | tf_op jit(solution)/shard_map/dot_general | solution.py:94
  125.0 0.0 reduce-scatter.2.cloned.1.call-update
  125.0 2.8 %copy.39 = f32[1,96,4096]{2,1,0:T(8,128)} copy(f32[1,96,4096]{1,2,0:T(8,128)} %bitcast.53) | data formatting | bytes 3145728 | tf_op jit(solution)/shard_map/stack;reshape | solution.py:41
  127.8 2.9 %copy.40 = f32[1,96,4096]{2,1,0:T(8,128)} copy(f32[1,96,4096]{1,2,0:T(8,128)} %bitcast.52) | data formatting | bytes 3145728 | tf_op jit(solution)/shard_map/stack;reshape | solution.py:41
  130.7 2.4 %fusion.59 = f32[96,512]{1,0:T(8,128)S(1)} fusion(bf16[96,2048]{1,0:T(8,128)(2,1)S(1)} %copy-done.5, bf16[2048,512]{1,0:T(8,128)(2,1)} %param.35), kind=kOutput, calls=%fused_computation.80 | convolution fusion | flops 201326592 | bytes 2686976 | tf_op jit(solution)/shard_map/dot_general | solution.py:132
  133.1 3.4 %pad_maximum_fusion = f32[2,96,4096]{2,1,0:T(8,128)} fusion(f32[1,96,4096]{2,1,0:T(8,128)} %copy.40, f32[1,96,4096]{2,1,0:T(8,128)S(1)} %copy-done.4), kind=kLoop, calls=%fused_computation.3 | loop fusion | flops 786432 | bytes 6291456 | tf_op jit(solution)/shard_map/stack | solution.py:41
  136.5 72.4 %reduce-scatter.2.cloned.1.call-done = bf16[96,2048]{1,0:T(8,128)(2,1)} async-done(((bf16[1536,2048]{1,0:T(8,128)(2,1)}), bf16[96,2048]{1,0:T(8,128)(2,1)}) %reduce-scatter.2.cloned.1.call-update) | async-done | bytes 393232 | tf_op jit(solution)/shard_map/reduce_scatter | solution.py:97
  208.9 3.9 %fusion.3 = bf16[96,2048]{1,0:T(8,128)(2,1)} fusion(bf16[512,2048]{1,0:T(8,128)(2,1)} %param.37, bf16[96,2048]{1,0:T(8,128)(2,1)S(1)} %copy-done.5, bf16[2048,512]{1,0:T(8,128)(2,1)} %param.36, f32[96,2048]{1,0:T(8,128)S(1)} %get-tuple-element.11, bf16[96,2048]{1,0:T(8,128)(2,1)} %reduce-scatter.2.cloned.1.call-done, f32[96,512]{1,0:T(8,128)S(1)} %fusion.59), kind=kOutput, calls=%fused_computation.8 | convolution fusion | flops 404127744 | bytes 6356992 | tf_op jit(solution)/shard_map/dot_general | solution.py:135
  (14 shorter events, 0.1 us)
Async XLA Ops:
  7.2 106.0 %copy-start = (bf16[1,512,2048]{2,1,0:T(8,128)(2,1)S(1)}, bf16[1,512,2048]{2,1,0:T(8,128)(2,1)}, u32[]{:S(2)}) copy-start(bf16[1,512,2048]{2,1,0:T(8,128)(2,1)} %param.34) | copy-start | bytes 6291460
  7.2 97.5 %all-gather.4.cloned.1.call-start = ((), (), s32[]{:S(2)}) async-start(), calls=%async_computation.1 | async-start | bytes 6684672 | tf_op jit(solution)/shard_map/all_gather | solution.py:90
  22.0 3.0 %copy-start.8 = (f32[64,64]{1,0:T(8,128)S(1)}, f32[64,64]{1,0:T(8,128)}, u32[]{:S(2)}) copy-start(f32[64,64]{1,0:T(8,128)} %param.25) | copy-start | bytes 49156
  22.0 3.0 %copy-start.9 = (f32[64,64]{1,0:T(8,128)S(1)}, f32[64,64]{1,0:T(8,128)}, u32[]{:S(2)}) copy-start(f32[64,64]{1,0:T(8,128)} %param.24) | copy-start | bytes 49156
  22.0 3.3 %copy-start.3 = (f32[1,96,4096]{1,2,0:T(8,128)S(1)}, f32[1,96,4096]{1,2,0:T(8,128)}, u32[]{:S(2)}) copy-start(f32[1,96,4096]{1,2,0:T(8,128)} %copy.35) | copy-start | bytes 4718596
  25.3 5.7 %copy-start.7 = (f32[2,64,16,64]{3,2,1,0:T(8,128)S(1)}, f32[2,64,16,64]{3,2,1,0:T(8,128)}, u32[]{:S(2)}) copy-start(f32[2,64,16,64]{3,2,1,0:T(8,128)} %param.28) | copy-start | bytes 1572868
  31.0 3.9 %copy-start.1 = (f32[96,64,64]{0,2,1:T(8,128)}, f32[96,64,64]{0,2,1:T(8,128)S(1)}, u32[]{:S(2)}) copy-start(f32[96,64,64]{0,2,1:T(8,128)S(1)} %get-tuple-element.2) | copy-start | bytes 4718596
  31.0 3.9 %copy-start.2 = (f32[96,64,64]{0,2,1:T(8,128)}, f32[96,64,64]{0,2,1:T(8,128)S(1)}, u32[]{:S(2)}) copy-start(f32[96,64,64]{0,2,1:T(8,128)S(1)} %get-tuple-element.3) | copy-start | bytes 4718596
  33.0 2.9 %copy-start.6 = (bf16[96,2048]{1,0:T(8,128)(2,1)S(1)}, bf16[96,2048]{1,0:T(8,128)(2,1)}, u32[]{:S(2)}) copy-start(bf16[96,2048]{1,0:T(8,128)(2,1)} %param.20) | copy-start | bytes 1179652
  33.0 2.9 %copy-start.13 = (f32[1024]{0:T(1024)S(1)}, f32[1024]{0:T(1024)}, u32[]{:S(2)}) copy-start(f32[1024]{0:T(1024)} %param.29) | copy-start | bytes 12292
  35.9 3.4 %copy-start.10 = (f32[2048]{0:T(1024)S(1)}, f32[2048]{0:T(1024)}, u32[]{:S(2)}) copy-start(f32[2048]{0:T(1024)} %param.31) | copy-start | bytes 24580
  35.9 4.3 %copy-start.11 = (s32[96,6]{0,1:T(8,128)S(1)}, s32[96,6]{0,1:T(8,128)}, u32[]{:S(2)}) copy-start(s32[96,6]{0,1:T(8,128)} %param.38) | copy-start | bytes 6916
  35.9 28.1 %copy-start.12 = (f32[96,6]{0,1:T(8,128)S(1)}, f32[96,6]{0,1:T(8,128)}, u32[]{:S(2)}) copy-start(f32[96,6]{0,1:T(8,128)} %param.39) | copy-start | bytes 6916
  40.2 168.7 %reduce-scatter.2.cloned.1.call-start = ((), (), s32[]{:S(2)}) async-start(), calls=%async_computation.2 | async-start | bytes 6684672 | tf_op jit(solution)/shard_map/reduce_scatter | solution.py:97
  127.8 2.9 %copy-start.5 = (bf16[96,2048]{1,0:T(8,128)(2,1)S(1)}, bf16[96,2048]{1,0:T(8,128)(2,1)}, u32[]{:S(2)}) copy-start(bf16[96,2048]{1,0:T(8,128)(2,1)} %multiply_convert_fusion.1) | copy-start | bytes 1179652
  130.7 2.4 %copy-start.4 = (f32[1,96,4096]{2,1,0:T(8,128)S(1)}, f32[1,96,4096]{2,1,0:T(8,128)}, u32[]{:S(2)}) copy-start(f32[1,96,4096]{2,1,0:T(8,128)} %copy.39) | copy-start | bytes 4718596
Sparse Core Ops, SparseCore 0:
  40.3 64.3 all-gather.3
  125.1 83.7 reduce-scatter.1

commit v2 on v1

--- a/solution.py
+++ b/solution.py
@@ -1,10 +1,14 @@
+import functools
 import jax
 import jax.numpy as jnp
 from jax import lax
+from jax.experimental import pallas as pl
+from jax.experimental.pallas import tpu as pltpu
 from jax.sharding import PartitionSpec as P
 
 norm_eps = 1e-06
 highest = lax.Precision.HIGHEST
+MESH = pl.DeviceIdType.MESH
 
 
 def root_scale(activations, scale_gain):
@@ -82,19 +86,395 @@
     return routed
 
 
-def gathered_experts(second_normed, routes, route_weights, expert_gate, expert_up, expert_down):
-    all_routes = lax.all_gather(routes, "ep", axis=0, tiled=True)
-    all_weights = lax.all_gather(route_weights, "ep", axis=0, tiled=True)
-    here = all_routes == lax.axis_index("ep")
-    weight = jnp.sum(jnp.where(here, all_weights, 0.0), axis=1)
-    rows = lax.all_gather(second_normed, "ep", axis=0, tiled=True)
-    gate_val = jnp.dot(rows, expert_gate[0], preferred_element_type=jnp.float32)
-    up_val = jnp.dot(rows, expert_up[0], preferred_element_type=jnp.float32)
-    hidden = (jax.nn.silu(gate_val) * up_val).astype(jnp.bfloat16)
-    piece = jnp.dot(hidden, expert_down[0], preferred_element_type=jnp.float32)
-    summed = lax.psum_scatter(piece.astype(jnp.bfloat16), "tp", scatter_dimension=1, tiled=True)
-    weighted = (weight[:, None] * summed.astype(jnp.float32)).astype(jnp.bfloat16)
-    return lax.psum_scatter(weighted, "ep", scatter_dimension=0, tiled=True).astype(jnp.float32)
+def near_first(extent):
+    return [sorted(range(extent), key=lambda other: (abs(other - at), other)) for at in range(extent)]
+
+
+def looked_up(table, position):
+    found = jnp.int32(0)
+    for at, entry in enumerate(table):
+        found = jnp.where(position == at, jnp.int32(entry), found)
+    return found
+
+
+def expert_kernel(
+    grid_shape, pieces,
+    own, middle, weights, gate_in, up_in, down_in, sgate_in, sup_in, sdown_in,
+    out,
+    rows_all, back, from_twin, from_side, from_far, weight_all,
+    gate, up, down, sgate, sup, sdown, hidden, shared, total,
+    load_sem, row_recv, own_z_send, fwd_z_send, fwd_x_send, fwd_twin_send,
+    w_send, w_recv, twin_send, twin_recv, side_send, side_recv, far_send, far_recv,
+):
+    zs, xs, cs = grid_shape
+    count = zs * xs * cs
+    me = lax.axis_index("ep")
+    core = lax.rem(me, cs)
+    col = lax.rem(me // cs, xs)
+    level = me // (cs * xs)
+    rows, width = own.shape
+    span = rows // pieces
+    hid = gate.shape[1]
+
+    def device(z, x, c):
+        return (z * xs + x) * cs + c
+
+    twin = device(level, col, 1 - core)
+    side = device(level, 1 - col, core)
+    order = [looked_up([row[j] for row in near_first(zs)], level) for j in range(zs)]
+
+    def part(base, h):
+        return pl.ds(pl.multiple_of(base * rows + h * span, 16), span)
+
+    loads = [
+        pltpu.make_async_copy(src, dst, load_sem.at[n])
+        for n, (src, dst) in enumerate(
+            ((sgate_in, sgate), (sup_in, sup), (sdown_in, sdown),
+             (gate_in.at[0], gate), (up_in.at[0], up), (down_in.at[0], down))
+        )
+    ]
+    for load in loads:
+        load.start()
+
+    barrier = pltpu.get_barrier_semaphore()
+    for step in range(1, count):
+        pl.semaphore_signal(
+            barrier, inc=1, device_id={"ep": lax.rem(me + step, count)}, device_id_type=MESH
+        )
+    pl.semaphore_wait(barrier, count - 1)
+
+    def remote(src, dst, send, recv, target):
+        return pltpu.make_async_remote_copy(
+            src_ref=src, dst_ref=dst, send_sem=send, recv_sem=recv,
+            device_id={"ep": target}, device_id_type=MESH,
+        )
+
+    sent = []
+
+    def push(src, dst, send, recv, target):
+        copy = remote(src, dst, send, recv, target)
+        copy.start()
+        sent.append(copy)
+
+    def row_copy(src_ref, src_rows, origin, h, send, target):
+        return remote(
+            src_ref.at[src_rows], rows_all.at[part(origin, h)], send, row_recv.at[origin, h], target
+        )
+
+    for h in range(pieces):
+        piece = pl.ds(h * span, span)
+
+        @pl.when(level > 0)
+        def _():
+            row_copy(own, piece, me, h, own_z_send.at[0, h], device(level - 1, col, core)).start()
+
+        @pl.when(level < zs - 1)
+        def _():
+            row_copy(own, piece, me, h, own_z_send.at[1, h], device(level + 1, col, core)).start()
+
+        for send, target in ((fwd_x_send.at[0, h], side), (fwd_twin_send.at[0, h], twin)):
+            copy = row_copy(own, piece, me, h, send, target)
+            copy.start()
+            sent.append(copy)
+
+    for step in range(1, count):
+        other = lax.rem(me + step, count)
+        push(
+            weights.at[other], weight_all.at[me], w_send.at[step], w_recv.at[count - step], other
+        )
+    rows_all[part(me, 0), :] = own[pl.ds(0, span), :]
+    for h in range(1, pieces):
+        rows_all[part(me, h), :] = own[pl.ds(h * span, span), :]
+    weight_all[me] = weights[me]
+
+    def arrived(origin, h):
+        row_copy(own, pl.ds(h * span, span), origin, h, own_z_send.at[0, h], twin).wait_recv()
+
+    def feed(source, take, gate_w, up_w, down_w, finish):
+        def first(n, carry):
+            cols = pl.ds(pl.multiple_of(n * 256, 256), 256)
+            data = source()
+            g = jnp.dot(data, gate_w[:, cols], preferred_element_type=jnp.float32)
+            u = jnp.dot(data, up_w[:, cols], preferred_element_type=jnp.float32)
+            hidden[pl.ds(0, take), cols] = (jax.nn.silu(g) * u).astype(jnp.bfloat16)
+            return carry
+
+        lax.fori_loop(0, hid // 256, first, 0)
+
+        def second(n, carry):
+            cols = pl.ds(pl.multiple_of(n * 512, 512), 512)
+            piece = jnp.dot(
+                hidden[pl.ds(0, take), :], down_w[:, cols], preferred_element_type=jnp.float32
+            )
+            finish(cols, piece.astype(jnp.bfloat16))
+            return carry
+
+        lax.fori_loop(0, width // 512, second, 0)
+
+    def chip(label, z, x):
+        base = device(z, x, 0)
+        block = pl.ds(pl.multiple_of(base * rows, 16), cs * rows)
+        scales = []
+        for c in range(cs):
+            line = jnp.broadcast_to(weight_all[base + c], (128, 128))
+            scales.append(jnp.transpose(line)[:rows])
+        scale = jnp.concatenate(scales, axis=0)
+        scale = jnp.concatenate([scale] * 4, axis=1)
+
+        def finish(cols, piece):
+            back[block, cols] = (piece.astype(jnp.float32) * scale).astype(jnp.bfloat16)
+
+        feed(lambda: rows_all[block, :], cs * rows, gate, up, down, finish)
+        push(
+            back.at[part_all(device(z, x, 1 - core))],
+            from_twin.at[label],
+            twin_send.at[label],
+            twin_recv.at[label],
+            twin,
+        )
+
+    def part_all(origin):
+        return pl.ds(pl.multiple_of(origin * rows, 16), rows)
+
+    for load in loads[:3]:
+        load.wait()
+
+    def keep(cols, piece):
+        shared[:, cols] = piece
+
+    feed(lambda: own[...], rows, sgate, sup, sdown, keep)
+    for load in loads[3:]:
+        load.wait()
+    for step in range(1, count):
+        remote(
+            weights.at[me], weight_all.at[lax.rem(me + step, count)],
+            w_send.at[step], w_recv.at[step], twin,
+        ).wait_recv()
+
+    def pair_in(z, x):
+        for h in range(pieces):
+            arrived(device(z, x, 1 - core), h)
+
+    pair_in(level, col)
+    chip(0, level, col)
+    for j in range(1, zs + 1):
+        if j < zs:
+            origin_z = order[j]
+            origin = device(origin_z, col, core)
+            for h in range(pieces):
+                arrived(origin, h)
+                onward = jnp.where(origin_z < level, level + 1, level - 1)
+
+                @pl.when((onward >= 0) & (onward < zs))
+                def _():
+                    row_copy(
+                        rows_all, part(origin, h), origin, h, fwd_z_send.at[j, h],
+                        device(onward, col, core),
+                    ).start()
+
+                for send, target in ((fwd_x_send.at[j, h], side), (fwd_twin_send.at[j, h], twin)):
+                    copy = row_copy(rows_all, part(origin, h), origin, h, send, target)
+                    copy.start()
+                    sent.append(copy)
+        across = device(order[j - 1], 1 - col, core)
+        for h in range(pieces):
+            arrived(across, h)
+            copy = row_copy(
+                rows_all, part(across, h), across, h, fwd_twin_send.at[zs + j - 1, h], twin
+            )
+            copy.start()
+            sent.append(copy)
+        if j < zs:
+            pair_in(order[j], col)
+            chip(j, order[j], col)
+        pair_in(order[j - 1], 1 - col)
+        chip(zs + j - 1, order[j - 1], 1 - col)
+
+    def twin_in(label):
+        remote(
+            from_twin.at[label], from_twin.at[label], twin_send.at[label], twin_recv.at[label], twin
+        ).wait_recv()
+
+    def added(first, others, store):
+        def strip(n, carry):
+            at = pl.multiple_of(n * 16, 16)
+            value = first(at).astype(jnp.float32)
+            for other in others:
+                value = value + other(at).astype(jnp.float32)
+            store(at, value)
+            return carry
+
+        lax.fori_loop(0, span // 16, strip, 0)
+
+    def back_at(origin, h):
+        return lambda at: back[pl.ds(pl.multiple_of(origin * rows + h * span + at, 16), 16), :]
+
+    def slot_at(ref, slot, h):
+        return lambda at: ref[slot, pl.ds(pl.multiple_of(h * span + at, 16), 16), :]
+
+    def to_back(origin, h):
+        def store(at, value):
+            back[pl.ds(pl.multiple_of(origin * rows + h * span + at, 16), 16), :] = value.astype(
+                jnp.bfloat16
+            )
+
+        return store
+
+    for j in reversed(range(zs)):
+        twin_in(zs + j)
+        origin = device(order[j], 1 - col, core)
+        for h in range(pieces):
+            added(back_at(origin, h), [slot_at(from_twin, zs + j, h)], to_back(origin, h))
+            push(
+                back.at[part(origin, h)], from_side.at[j, pl.ds(h * span, span)],
+                side_send.at[j, h], side_recv.at[j, h], side,
+            )
+
+    def side_in(j, h):
+        view = from_side.at[j, pl.ds(h * span, span)]
+        remote(view, view, side_send.at[j, h], side_recv.at[j, h], side).wait_recv()
+
+    def far_in(slot, h):
+        view = from_far.at[slot, pl.ds(h * span, span)]
+        remote(view, view, far_send.at[0, h], far_recv.at[slot, h], side).wait_recv()
+
+    for j in reversed(range(1, zs)):
+        twin_in(j)
+        goal = order[j]
+        origin = device(goal, col, core)
+        nearer = jnp.where(goal < level, level - 1, level + 1)
+        behind = jnp.where(goal < level, level + 1, level - 1)
+        slot = jnp.where((nearer == goal) & (goal > level), zs, goal)
+        for h in range(pieces):
+            side_in(j, h)
+            terms = [slot_at(from_twin, j, h), slot_at(from_side, j, h)]
+
+            @pl.when((behind >= 0) & (behind < zs))
+            def _():
+                far_in(goal, h)
+                added(
+                    back_at(origin, h), terms + [slot_at(from_far, goal, h)], to_back(origin, h)
+                )
+
+            @pl.when((behind < 0) | (behind >= zs))
+            def _():
+                added(back_at(origin, h), terms, to_back(origin, h))
+
+            push(
+                back.at[part(origin, h)], from_far.at[slot, pl.ds(h * span, span)],
+                far_send.at[j, h], far_recv.at[slot, h], device(nearer, col, core),
+            )
+    twin_in(0)
+    for h in range(pieces):
+        side_in(0, h)
+
+        def to_total(at, value):
+            total[pl.ds(pl.multiple_of(h * span + at, 16), 16), :] = value
+
+        def total_at(at):
+            return total[pl.ds(pl.multiple_of(h * span + at, 16), 16), :]
+
+        added(back_at(me, h), [slot_at(from_twin, 0, h), slot_at(from_side, 0, h)], to_total)
+
+        @pl.when(level > 0)
+        def _():
+            far_in(zs, h)
+            added(total_at, [slot_at(from_far, zs, h)], to_total)
+
+        @pl.when(level < zs - 1)
+        def _():
+            far_in(level, h)
+            added(total_at, [slot_at(from_far, level, h)], to_total)
+
+        def plain(ref):
+            return lambda at: ref[pl.ds(pl.multiple_of(h * span + at, 16), 16), :]
+
+        def to_out(at, value):
+            out[pl.ds(pl.multiple_of(h * span + at, 16), 16), :] = value.astype(jnp.bfloat16)
+
+        added(plain(middle), [total_at, plain(shared)], to_out)
+
+    for copy in sent:
+        copy.wait_send()
+    for h in range(pieces):
+        piece = pl.ds(h * span, span)
+
+        @pl.when(level > 0)
+        def _():
+            row_copy(own, piece, me, h, own_z_send.at[0, h], twin).wait_send()
+
+        @pl.when(level < zs - 1)
+        def _():
+            row_copy(own, piece, me, h, own_z_send.at[1, h], twin).wait_send()
+
+        for j in range(1, zs):
+            onward = jnp.where(order[j] < level, level + 1, level - 1)
+
+            @pl.when((onward >= 0) & (onward < zs))
+            def _():
+                row_copy(own, piece, me, h, fwd_z_send.at[j, h], twin).wait_send()
+
+
+def expert_stage(
+    second_normed, middle, routes, route_weights,
+    expert_gate, expert_up, expert_down, shared_gate, shared_up, shared_down,
+):
+    experts = lax.axis_size("ep")
+    grid_shape = (experts // 4, 2, 2)
+    zs = grid_shape[0]
+    rows, width = second_normed.shape
+    hid = expert_gate.shape[2]
+    pieces = 2 if rows % 32 == 0 else 1
+    chosen = routes[None, :, :] == jnp.arange(experts, dtype=jnp.int32)[:, None, None]
+    weights = jnp.sum(jnp.where(chosen, route_weights[None], 0.0), axis=2)
+    weights = jnp.pad(weights, ((0, 0), (0, 128 - rows)))[:, None, :]
+    vmem = pl.BlockSpec(memory_space=pltpu.VMEM)
+    hbm = pl.BlockSpec(memory_space=pl.ANY)
+    dma = pltpu.SemaphoreType.DMA
+    half = jnp.bfloat16
+    return pl.pallas_call(
+        functools.partial(expert_kernel, grid_shape, pieces),
+        out_shape=jax.ShapeDtypeStruct((rows, width), half),
+        in_specs=[vmem] * 3 + [hbm] * 6,
+        out_specs=vmem,
+        scratch_shapes=[
+            pltpu.VMEM((experts * rows, width), half),
+            pltpu.VMEM((experts * rows, width), half),
+            pltpu.VMEM((2 * zs, rows, width), half),
+            pltpu.VMEM((zs, rows, width), half),
+            pltpu.VMEM((zs + 1, rows, width), half),
+            pltpu.VMEM((experts, 1, 128), jnp.float32),
+            pltpu.VMEM((width, hid), half),
+            pltpu.VMEM((width, hid), half),
+            pltpu.VMEM((hid, width), half),
+            pltpu.VMEM(shared_gate.shape, half),
+            pltpu.VMEM(shared_up.shape, half),
+            pltpu.VMEM(shared_down.shape, half),
+            pltpu.VMEM((2 * rows, hid), half),
+            pltpu.VMEM((rows, width), half),
+            pltpu.VMEM((rows, width), jnp.float32),
+            dma((6,)),
+            dma((experts, pieces)),
+            dma((2, pieces)),
+            dma((zs, pieces)),
+            dma((zs, pieces)),
+            dma((2 * zs, pieces)),
+            dma((experts,)),
+            dma((experts,)),
+            dma((2 * zs,)),
+            dma((2 * zs,)),
+            dma((zs, pieces)),
+            dma((zs, pieces)),
+            dma((zs, pieces)),
+            dma((zs + 1, pieces)),
+        ],
+        compiler_params=pltpu.CompilerParams(
+            collective_id=0, has_side_effects=True, vmem_limit_bytes=60 * 1024 * 1024
+        ),
+    )(
+        second_normed, middle, weights,
+        expert_gate, expert_up, expert_down, shared_gate, shared_up, shared_down,
+    )
 
 
 def body(
@@ -129,6 +509,12 @@
     mixer_out = lax.psum(partial_value.astype(jnp.bfloat16), "tp").astype(jnp.float32)
     middle = (tokens.astype(jnp.float32) + mixer_out).astype(jnp.bfloat16)
     second_normed = root_scale(middle, channel_gain)
+    if lax.axis_size("tp") == 1 and lax.axis_size("ep") == 16:
+        layer_out = expert_stage(
+            second_normed, middle, routes, route_weights,
+            expert_gate, expert_up, expert_down, shared_gate, shared_up, shared_down,
+        )
+        return (layer_out, new_state)
     shared_gval = jnp.dot(second_normed, shared_gate, preferred_element_type=jnp.float32)
     shared_uval = jnp.dot(second_normed, shared_up, preferred_element_type=jnp.float32)
     shared_hidden = (jax.nn.silu(shared_gval) * shared_uval).astype(jnp.bfloat16)
@@ -136,16 +522,10 @@
     shared_out = lax.psum_scatter(
         shared_piece.astype(jnp.bfloat16), "tp", scatter_dimension=1, tiled=True
     ).astype(jnp.float32)
-    experts = lax.axis_size("ep")
     half_cols = second_normed.shape[1] // lax.axis_size("tp")
-    if experts <= 16:
-        routed = gathered_experts(
-            second_normed, routes, route_weights, expert_gate, expert_up, expert_down
-        )
-    else:
-        routed = exchanged_experts(
-            second_normed, routes, route_weights, expert_gate, expert_up, expert_down
-        )
+    routed = exchanged_experts(
+        second_normed, routes, route_weights, expert_gate, expert_up, expert_down
+    )
     own_middle = lax.dynamic_slice_in_dim(middle, lax.axis_index("tp") * half_cols, half_cols, 1)
     layer_out = (own_middle.astype(jnp.float32) + routed + shared_out).astype(jnp.bfloat16)
     return (layer_out, new_state)

time: 220 us -> 141 us (0.64)
  Pallas kernels: 0 us -> 97.1 us
  waiting for transfers between devices: 94.8 us -> 0 us
  blocking collectives: 42 us -> 0 us
  matrix products: 45.6 us -> 19.7 us
  between operations: 14.2 us -> 0.77 us
    pallas_call x0 -> x1, Pallas kernels: none -> 97.1 us  [expert_stage(): pl.pallas_call(functools.partial(expert_kernel, grid_shape, pieces), out_...]
    reduce_scatter x1 -> x0, waiting for transfers between devices: 72.4 us -> none  [gathered_experts(): lax.psum_scatter(weighted, 'ep', scatter_dimension=0, tiled=True)]
    all_gather x2 -> x0, blocking collectives: 42 us -> none  [the longest x1 23.8 us: gathered_experts(): all_routes = lax.all_gather(routes, 'ep', axis=0, tiled=True)]
    dot_general x4 -> x0, matrix products: 26.6 us -> none  [the longest x1 11.8 us: gathered_experts(): piece = jnp.dot(hidden, expert_down[0], preferred_element_type=jnp.float32)]
    all_gather x1 -> x0, waiting for transfers between devices: 22.4 us -> none  [gathered_experts(): rows = lax.all_gather(second_normed, 'ep', axis=0, tiled=True)]
  transfers between devices with their start and end apart: 2 -> 0, of which waited for: 2 -> 0; matrix products, arithmetic and copies ran while one was open for 5% -> 0% of each run, Pallas kernels for 0% -> 0%
where the time goes in v2:
time: 141 us; the launch traced here: 140 us
  Pallas kernels  97.1 us (69%)
  matrix products  19.7 us (14%)
  local copies, waits for them, and re-layouts  15.6 us (11%)
  other arithmetic  7 us (5%)
    pallas_call x1, Pallas kernels, expert_stage(): pl.pallas_call(functools.partial(expert_kernel, grid_shape, pieces), out_...  97.1 us
    slice x2, local copies, waits for them, and re-layouts, state_update(): old_real = prior_state[0].reshape(sequences, groups, -1)  6.19 us
    dot_general x1, matrix products, state_update(): jnp.einsum('sgh,gph->sgp', driven, input_map[1], precision=highest)  6.17 us
    another operation x2, local copies, waits for them, and re-layouts, state_update(): jnp.stack([fresh_real.reshape(sequences, -1), fresh_imag.reshape(sequence...  4.47 us
    another operation x1, other arithmetic, state_update(): jnp.stack([fresh_real.reshape(sequences, -1), fresh_imag.reshape(sequence...  3.9 us
    dot_general x1, matrix products, body(): jnp.dot(activated, out_weight, preferred_element_type=jnp.float32)  3.33 us
    dot_general x1, matrix products, body(): jnp.dot(normed, in_weight, preferred_element_type=jnp.float32)  3.26 us
    dot_general x1, matrix products, state_update(): jnp.einsum('sgh,gph->sgp', driven, input_map[0], precision=highest)  3.15 us

profile of v2, /device:TPU:0, one launch (start us, length us, event | category | flops | bytes accessed | tf_op | source)
XLA Modules:
  0.0 140.3 jit_solution(14462307054845925612)
XLA Ops:
  0.6 0.7 exp.6
  1.3 1.0 cosine_multiply_fusion
  2.3 1.2 fusion.6
  3.5 0.0 copy-start.4
  3.5 3.3 %convolution_convert_fusion.1 = bf16[96,1024]{1,0:T(8,128)(2,1)S(1)} fusion(bf16[2048,1024]{1,0:T(8,128)(2,1)} %param.23, bf16[96,2048]{1,0:T(8,128)(2,1)} %param.20, f32[2048]{0:T(1024)} %param.22, f32[96]{0:T(128)S(1)} %add_rsqrt_fusion.1), kind=kOutput, calls=%fused_computation.10 | convolution fusion | flops 403537920 | bytes 4792704 | tf_op jit(solution)/shard_map/dot_general | solution.py:503
  6.8 0.2 copy.41
  6.9 0.0 copy-done.4
  6.9 3.1 %fusion.14 = f32[64,96,64]{1,2,0:T(8,128)} fusion(bf16[96,64,16]{0,2,1:T(8,128)(2,1)S(1)} %bitcast.37, f32[2,64,64,16]{2,3,1,0:T(8,128)S(1)} %copy-done.4), kind=kOutput, calls=%fused_computation.25 | convolution fusion | flops 75497472 | bytes 2359296 | tf_op jit(solution)/shard_map/sgh,gph->sgp/dot_general | solution.py:34
  10.1 3.3 %fusion.41 = (f32[1,96,4096]{2,1,0:T(8,128)}, f32[1,96,4096]{2,1,0:T(8,128)S(1)}) fusion(f32[2,96,4096]{2,1,0:T(8,128)} %param.21), kind=kLoop, calls=%fused_computation.60 | loop fusion | bytes 6291456 | tf_op jit(solution)/shard_map/slice | solution.py:38
  13.4 2.8 %copy.39 = f32[1,96,4096]{1,2,0:T(8,128)} copy(f32[1,96,4096]{2,1,0:T(8,128)} %get-tuple-element.4) | data formatting | bytes 3145728 | tf_op jit(solution)/shard_map/slice | solution.py:38
  16.3 1.8 %copy.40 = f32[1,96,4096]{1,2,0:T(8,128)} copy(f32[1,96,4096]{2,1,0:T(8,128)S(1)} %get-tuple-element.5) | data formatting | bytes 3145728 | tf_op jit(solution)/shard_map/slice | solution.py:39
  18.1 0.0 copy-start.5
  18.1 6.2 %bitcast_add_fusion = (f32[96,64,64]{0,2,1:T(8,128)S(1)}, f32[96,64,64]{0,2,1:T(8,128)S(1)}) fusion(f32[64,96,64]{1,2,0:T(8,128)} %fusion.14, f32[96,64,64]{0,2,1:T(8,128)} %bitcast.35, f32[96,64,64]{0,2,1:T(8,128)} %bitcast.36, f32[64,64]{1,0:T(8,128)S(1)} %get-tuple-element.8, f32[64,64]{1,0:T(8,128)S(1)} %get-tuple-element.7, ...), kind=kOutput, calls=%fused_computation.5 | convolution fusion | flops 81002496 | bytes 10223616 | tf_op jit(solution)/shard_map/sgh,gph->sgp/dot_general | solution.py:35
  24.2 0.0 copy-start
  24.3 0.0 copy-done.5
  24.3 1.9 %fusion.10 = f32[64,96,16]{1,2,0:T(8,128)S(1)} fusion(f32[96,64,64]{0,2,1:T(8,128)S(1)} %get-tuple-element.3, f32[2,64,16,64]{3,2,1,0:T(8,128)S(1)} %copy-done.5), kind=kOutput, calls=%fused_computation.21 | convolution fusion | flops 75497472 | bytes 3014656 | tf_op jit(solution)/shard_map/ghp,sgp->sgh/dot_general | solution.py:42
  26.2 0.0 copy-start.2
  26.2 0.0 copy-start.7
  26.2 1.9 %convolution_subtract_fusion = f32[64,96,16]{1,2,0:T(8,128)S(1)} fusion(f32[64,96,16]{1,2,0:T(8,128)S(1)} %fusion.10, f32[96,64,64]{0,2,1:T(8,128)S(1)} %get-tuple-element.2, f32[2,64,16,64]{3,2,1,0:T(8,128)S(1)} %copy-done.5), kind=kOutput, calls=%fused_computation.7 | convolution fusion | flops 75595776 | bytes 3538944 | tf_op jit(solution)/shard_map/ghp,sgp->sgh/dot_general | solution.py:43
  28.1 0.0 copy-done
  28.1 0.9 copy.42
  29.1 0.0 copy-done.2
  29.1 0.0 copy-done.7
  29.1 0.0 copy-start.6
  29.1 0.0 copy-start.8
  29.1 0.0 copy-start.9
  29.1 3.3 %fusion.3 = (f32[96]{0:T(128)S(1)}, bf16[96,2048]{1,0:T(8,128)(2,1)S(1)}) fusion(bf16[1024,2048]{1,0:T(8,128)(2,1)} %param.30, f32[96,1024]{1,0:T(8,128)} %copy.42, bf16[96,1024]{1,0:T(8,128)(2,1)S(1)} %convolution_convert_fusion.1, f32[1024]{0:T(1024)S(1)} %copy-done.7, bf16[96,2048]{1,0:T(8,128)(2,1)S(1)} %copy-done.2), kind=kOutput, calls=%fused_computation.13 | convolution fusion | flops 405405600 | bytes 5575040 | tf_op jit(solution)/shard_map/dot_general | solution.py:508
  32.4 0.0 copy-start.1
  32.4 0.0 copy-done.6
  32.5 0.9 fusion.5.own
  33.4 0.0 copy-done.8
  33.4 0.0 copy-done.9
  33.4 0.6 pad.4
  34.0 0.0 copy-done.1
  34.0 97.1 %shard_map.203 = bf16[96,2048]{1,0:T(8,128)(2,1)} custom-call(bf16[96,2048]{1,0:T(8,128)(2,1)} %fusion.5.own, bf16[96,2048]{1,0:T(8,128)(2,1)} %copy-done.1, f32[16,1,128]{2,1,0:T(1,128)} %bitcast.40, bf16[1,2048,512]{2,1,0:T(8,128)(2,1)} %gate_in.1, bf16[1,2048,512]{2,1,0:T(8,128)(2,1)} %up_in.1, bf16[1,512,2048]{2,1,0:T(8,128)(2,1)} %down_in.1, ...), custom_call_target="tpu_custom_call" | custom-call | tf_op jit(solution)/shard_map/pallas_call | solution.py:435
  131.1 2.8 %copy.43 = f32[1,96,4096]{2,1,0:T(8,128)} copy(f32[1,96,4096]{1,2,0:T(8,128)} %bitcast.34) | data formatting | bytes 3145728 | tf_op jit(solution)/shard_map/stack;reshape | solution.py:45
  133.9 1.7 %copy.44 = f32[1,96,4096]{2,1,0:T(8,128)} copy(f32[1,96,4096]{1,2,0:T(8,128)S(1)} %bitcast.33) | data formatting | bytes 3145728 | tf_op jit(solution)/shard_map/stack;reshape | solution.py:45
  135.6 0.0 copy-start.3
  135.6 3.9 %pad_maximum_fusion = f32[2,96,4096]{2,1,0:T(8,128)} fusion(f32[1,96,4096]{2,1,0:T(8,128)} %copy.44, f32[1,96,4096]{2,1,0:T(8,128)} %copy.43), kind=kLoop, calls=%fused_computation | loop fusion | flops 786432 | bytes 6291456 | tf_op jit(solution)/shard_map/stack | solution.py:45
  139.5 0.0 copy-done.3
  139.5 0.7 copy.46
  (3 shorter events, 0.0 us)
Async XLA Ops:
  3.5 3.5 %copy-start.4 = (f32[2,64,64,16]{2,3,1,0:T(8,128)S(1)}, f32[2,64,64,16]{2,3,1,0:T(8,128)}, u32[]{:S(2)}) copy-start(f32[2,64,64,16]{2,3,1,0:T(8,128)} %param.27) | copy-start | bytes 1572868
  18.1 6.2 %copy-start.5 = (f32[2,64,16,64]{3,2,1,0:T(8,128)S(1)}, f32[2,64,16,64]{3,2,1,0:T(8,128)}, u32[]{:S(2)}) copy-start(f32[2,64,16,64]{3,2,1,0:T(8,128)} %param.28) | copy-start | bytes 1572868
  24.2 3.9 %copy-start = (f32[96,64,64]{0,2,1:T(8,128)}, f32[96,64,64]{0,2,1:T(8,128)S(1)}, u32[]{:S(2)}) copy-start(f32[96,64,64]{0,2,1:T(8,128)S(1)} %get-tuple-element.3) | copy-start | bytes 4718596
  26.2 2.9 %copy-start.2 = (bf16[96,2048]{1,0:T(8,128)(2,1)S(1)}, bf16[96,2048]{1,0:T(8,128)(2,1)}, u32[]{:S(2)}) copy-start(bf16[96,2048]{1,0:T(8,128)(2,1)} %param.20) | copy-start | bytes 1179652
  26.2 2.9 %copy-start.7 = (f32[1024]{0:T(1024)S(1)}, f32[1024]{0:T(1024)}, u32[]{:S(2)}) copy-start(f32[1024]{0:T(1024)} %param.29) | copy-start | bytes 12292
  29.1 3.4 %copy-start.6 = (f32[2048]{0:T(1024)S(1)}, f32[2048]{0:T(1024)}, u32[]{:S(2)}) copy-start(f32[2048]{0:T(1024)} %param.31) | copy-start | bytes 24580
  29.1 4.3 %copy-start.8 = (f32[96,6]{0,1:T(8,128)S(1)}, f32[96,6]{0,1:T(8,128)}, u32[]{:S(2)}) copy-start(f32[96,6]{0,1:T(8,128)} %param.39) | copy-start | bytes 6916
  29.1 4.3 %copy-start.9 = (s32[96,6]{0,1:T(8,128)S(1)}, s32[96,6]{0,1:T(8,128)}, u32[]{:S(2)}) copy-start(s32[96,6]{0,1:T(8,128)} %param.38) | copy-start | bytes 6916
  32.4 1.6 %copy-start.1 = (bf16[96,2048]{1,0:T(8,128)(2,1)}, bf16[96,2048]{1,0:T(8,128)(2,1)S(1)}, u32[]{:S(2)}) copy-start(bf16[96,2048]{1,0:T(8,128)(2,1)S(1)} %get-tuple-element.11.middle) | copy-start | bytes 1179652
  135.6 3.9 %copy-start.3 = (bf16[96,2048]{1,0:T(8,128)(2,1)S(1)}, bf16[96,2048]{1,0:T(8,128)(2,1)}, u32[]{:S(2)}) copy-start(bf16[96,2048]{1,0:T(8,128)(2,1)} %shard_map.203) | copy-start | bytes 1179652

commit v3 on v2

--- a/solution.py
+++ b/solution.py
@@ -477,6 +477,144 @@
     )
 
 
+def mixer_kernel(
+    tokens, prior, mix_gain, in_weight, params, input_map, output_map, skip, out_weight,
+    channel_gain, new_state, middle, second, normed, acts, acc,
+):
+    step = pl.program_id(0)
+    lane = 128
+    channels = in_weight.shape[1]
+    width = input_map.shape[2]
+    group = acts.shape[1] * width // prior.shape[2]
+    per = lane // group
+    states = per * width
+
+    def scaled(values, gain):
+        factor = lax.rsqrt(jnp.mean(values * values, axis=-1, keepdims=True) + norm_eps)
+        return (values * factor * gain[...]).astype(jnp.bfloat16)
+
+    @pl.when(step == 0)
+    def _():
+        normed[...] = scaled(tokens[...].astype(jnp.float32), mix_gain)
+        acc[...] = jnp.zeros_like(acc)
+
+    drive = jnp.dot(normed[...], in_weight[...], preferred_element_type=jnp.float32)
+    drive = drive.astype(jnp.bfloat16)
+    row = lax.broadcasted_iota(jnp.int32, (lane, states), 0) // group
+    column = lax.broadcasted_iota(jnp.int32, (lane, states), 1) // width
+    own_group = row == column
+
+    def spread(table):
+        tiled = jnp.concatenate([table] * per, axis=1)
+        return jnp.where(own_group, tiled, 0.0).astype(jnp.bfloat16)
+
+    for sub in range(channels // lane):
+        cols = slice(sub * lane, (sub + 1) * lane)
+        ent = slice(sub * states, (sub + 1) * states)
+        part = drive[:, cols]
+        push_real = jnp.dot(
+            part, spread(input_map[0, cols, :]), preferred_element_type=jnp.float32
+        )
+        push_imag = jnp.dot(
+            part, spread(input_map[1, cols, :]), preferred_element_type=jnp.float32
+        )
+        turn_real, turn_imag = params[0:1, ent], params[1:2, ent]
+        hold_real, hold_imag = params[2:3, ent], params[3:4, ent]
+        old_real, old_imag = prior[0, :, ent], prior[1, :, ent]
+        fresh_real = (
+            turn_real * old_real - turn_imag * old_imag
+            + (push_real * hold_real - push_imag * hold_imag)
+        )
+        fresh_imag = (
+            turn_real * old_imag + turn_imag * old_real
+            + (push_real * hold_imag + push_imag * hold_real)
+        )
+        new_state[0, :, ent] = fresh_real
+        new_state[1, :, ent] = fresh_imag
+        across = (((1,), (1,)), ((), ()))
+        readout = lax.dot_general(
+            fresh_real.astype(jnp.bfloat16), spread(output_map[0, cols, :]), across,
+            preferred_element_type=jnp.float32,
+        ) - lax.dot_general(
+            fresh_imag.astype(jnp.bfloat16), spread(output_map[1, cols, :]), across,
+            preferred_element_type=jnp.float32,
+        )
+        readout = readout + skip[:, cols] * part.astype(jnp.float32)
+        acts[:, cols] = jax.nn.gelu(readout).astype(jnp.bfloat16)
+    acc[...] += jnp.dot(acts[...], out_weight[...], preferred_element_type=jnp.float32)
+
+    @pl.when(step == pl.num_programs(0) - 1)
+    def _():
+        mixed = acc[...].astype(jnp.bfloat16).astype(jnp.float32)
+        mid = (tokens[...].astype(jnp.float32) + mixed).astype(jnp.bfloat16)
+        middle[...] = mid
+        second[...] = scaled(mid.astype(jnp.float32), channel_gain)
+
+
+def mixer_stage(
+    tokens, prior_state, mix_gain, in_weight, decay_rate, frequency, log_step,
+    input_map, output_map, skip_gain, out_weight, channel_gain,
+):
+    rows, model = tokens.shape
+    groups, width = decay_rate.shape
+    channels = in_weight.shape[1]
+    step_size = jnp.exp(log_step)[:, None]
+    real_rate = -decay_rate
+    magnitude = jnp.exp(real_rate * step_size)
+    turn_real = magnitude * jnp.cos(frequency * step_size)
+    turn_imag = magnitude * jnp.sin(frequency * step_size)
+    denominator = real_rate * real_rate + frequency * frequency
+    hold_real = ((turn_real - 1.0) * real_rate + turn_imag * frequency) / denominator
+    hold_imag = (turn_imag * real_rate - (turn_real - 1.0) * frequency) / denominator
+    params = jnp.stack([turn_real, turn_imag, hold_real, hold_imag]).reshape(4, -1)
+    in_map = jnp.transpose(input_map, (0, 1, 3, 2)).reshape(2, channels, width)
+    out_map = output_map.reshape(2, channels, width)
+    block = 256
+    states = block * groups * width // channels
+
+    def whole(*shape):
+        return pl.BlockSpec(shape, lambda i: (0,) * len(shape))
+
+    half = jnp.bfloat16
+    return pl.pallas_call(
+        mixer_kernel,
+        grid=(channels // block,),
+        out_shape=(
+            jax.ShapeDtypeStruct(prior_state.shape, jnp.float32),
+            jax.ShapeDtypeStruct((rows, model), half),
+            jax.ShapeDtypeStruct((rows, model), half),
+        ),
+        in_specs=[
+            whole(rows, model),
+            pl.BlockSpec((2, rows, states), lambda i: (0, 0, i)),
+            whole(1, model),
+            pl.BlockSpec((model, block), lambda i: (0, i)),
+            pl.BlockSpec((4, states), lambda i: (0, i)),
+            pl.BlockSpec((2, block, width), lambda i: (0, i, 0)),
+            pl.BlockSpec((2, block, width), lambda i: (0, i, 0)),
+            pl.BlockSpec((1, block), lambda i: (0, i)),
+            pl.BlockSpec((block, model), lambda i: (i, 0)),
+            whole(1, model),
+        ],
+        out_specs=(
+            pl.BlockSpec((2, rows, states), lambda i: (0, 0, i)),
+            whole(rows, model),
+            whole(rows, model),
+        ),
+        scratch_shapes=[
+            pltpu.VMEM((rows, model), half),
+            pltpu.VMEM((rows, block), half),
+            pltpu.VMEM((rows, model), jnp.float32),
+        ],
+        compiler_params=pltpu.CompilerParams(
+            dimension_semantics=("arbitrary",), vmem_limit_bytes=62 * 1024 * 1024
+        ),
+    )(
+        tokens, prior_state, mix_gain[None], in_weight, params, in_map, out_map,
+        skip_gain[None], out_weight, channel_gain[None],
+    )
+
+
 def body(
     tokens,
     prior_state,
@@ -499,6 +637,16 @@
     routes,
     route_weights,
 ):
+    if lax.axis_size("tp") == 1 and lax.axis_size("ep") == 16:
+        new_state, middle, second_normed = mixer_stage(
+            tokens, prior_state, mix_gain, in_weight, decay_rate, frequency, log_step,
+            input_map, output_map, skip_gain, out_weight, channel_gain,
+        )
+        layer_out = expert_stage(
+            second_normed, middle, routes, route_weights,
+            expert_gate, expert_up, expert_down, shared_gate, shared_up, shared_down,
+        )
+        return (layer_out, new_state)
     normed = root_scale(tokens, mix_gain)
     drive_rows = jnp.dot(normed, in_weight, preferred_element_type=jnp.float32).astype(jnp.bfloat16)
     readout, new_state = state_update(
@@ -509,12 +657,6 @@
     mixer_out = lax.psum(partial_value.astype(jnp.bfloat16), "tp").astype(jnp.float32)
     middle = (tokens.astype(jnp.float32) + mixer_out).astype(jnp.bfloat16)
     second_normed = root_scale(middle, channel_gain)
-    if lax.axis_size("tp") == 1 and lax.axis_size("ep") == 16:
-        layer_out = expert_stage(
-            second_normed, middle, routes, route_weights,
-            expert_gate, expert_up, expert_down, shared_gate, shared_up, shared_down,
-        )
-        return (layer_out, new_state)
     shared_gval = jnp.dot(second_normed, shared_gate, preferred_element_type=jnp.float32)
     shared_uval = jnp.dot(second_normed, shared_up, preferred_element_type=jnp.float32)
     shared_hidden = (jax.nn.silu(shared_gval) * shared_uval).astype(jnp.bfloat16)

time: 141 us -> 114 us (0.81)
  matrix products: 19.7 us -> 0 us
  local copies, waits for them, and re-layouts: 15.6 us -> 3.36 us
  Pallas kernels: 97.1 us -> 108 us
  other arithmetic: 7 us -> 2.4 us
    dot_general x6 -> x0, matrix products: 19.7 us -> none  [the longest x1 6.17 us: state_update(): jnp.einsum('sgh,gph->sgp', driven, input_map[1], precision=highest)]
    pallas_call x0 -> x1, Pallas kernels: none -> 10.4 us  [mixer_stage(): pl.pallas_call(mixer_kernel, grid=(channels // block,), out_shape=(jax.Sh...]
    slice x3 -> x0, local copies, waits for them, and re-layouts: 7.97 us -> none  [the longest x2 6.19 us: state_update(): old_real = prior_state[0].reshape(sequences, groups, -1)]
    another operation x2 -> x4, local copies, waits for them, and re-layouts: 4.47 us -> 0.34 us  [mixer_stage(): jnp.stack([turn_real, turn_imag, hold_real, hold_imag]).reshape(4, -1)]
    another operation x1, other arithmetic: 3.9 us -> 0.69 us  [mixer_stage(): jnp.stack([turn_real, turn_imag, hold_real, hold_imag]).reshape(4, -1)]
where the time goes in v3:
time: 114 us
  Pallas kernels  108 us (95%)
  local copies, waits for them, and re-layouts  3.36 us (3%)
  other arithmetic  2.4 us (2%)
    pallas_call x1, Pallas kernels, expert_stage(): pl.pallas_call(functools.partial(expert_kernel, grid_shape, pieces), out_...  97.1 us
    pallas_call x1, Pallas kernels, mixer_stage(): pl.pallas_call(mixer_kernel, grid=(channels // block,), out_shape=(jax.Sh...  10.4 us

profile of v3, /device:TPU:0, one launch (start us, length us, event | category | flops | bytes accessed | tf_op | source)
XLA Modules:
  0.0 114.0 jit_solution(13221812668548476085)
XLA Ops:
  0.6 0.7 exp.6
  1.3 0.7 select_reduce_fusion
  2.0 0.6 pad.4
  2.6 1.0 cosine_multiply_fusion
  3.6 0.1 stack.15
  3.7 0.1 stack.17
  3.8 0.1 stack.18
  3.9 0.1 stack.16
  4.0 0.7 pad_maximum_fusion.params
  4.7 10.4 %shard_map.203 = (f32[2,96,4096]{2,1,0:T(8,128)}, bf16[96,2048]{1,0:T(8,128)(2,1)}, bf16[96,2048]{1,0:T(8,128)(2,1)}) custom-call(bf16[96,2048]{1,0:T(8,128)(2,1)} %tokens.1, f32[2,96,4096]{2,1,0:T(8,128)} %prior.1, f32[1,2048]{1,0:T(1,128)} %bitcast.11, bf16[2048,1024]{1,0:T(8,128)(2,1)} %in_weight.1, f32[4,4096]{1,0:T(4,128)} %pad_maximum_fusion.params, ...), custom_call_target="tpu_custom_call" | custom-call | tf_op jit(solution)/shard_map/pallas_call | solution.py:579
  15.0 97.1 %shard_map.204 = bf16[96,2048]{1,0:T(8,128)(2,1)} custom-call(bf16[96,2048]{1,0:T(8,128)(2,1)} %get-tuple-element.5.own, bf16[96,2048]{1,0:T(8,128)(2,1)} %get-tuple-element.6.middle, f32[16,1,128]{2,1,0:T(1,128)} %bitcast.10, bf16[1,2048,512]{2,1,0:T(8,128)(2,1)} %gate_in.1, bf16[1,2048,512]{2,1,0:T(8,128)(2,1)} %up_in.1, bf16[1,512,2048]{2,1,0:T(8,128)(2,1)} %down_in.1, ...), custom_call_target="tpu_custom_call" | custom-call | tf_op jit(solution)/shard_map/pallas_call | solution.py:435
  112.2 1.8 %copy.25 = bf16[96,2048]{1,0:T(8,128)(2,1)} copy(bf16[96,2048]{1,0:T(8,128)(2,1)} %shard_map.204) | data formatting | bytes 786432

commit v4 on v3

--- a/solution.py
+++ b/solution.py
@@ -87,7 +87,7 @@
 
 
 def near_first(extent):
-    return [sorted(range(extent), key=lambda other: (abs(other - at), other)) for at in range(extent)]
+    return [sorted(range(extent), key=lambda other: (abs(other - at), min(other, extent - 1 - other))) for at in range(extent)]
 
 
 def looked_up(table, position):
@@ -129,8 +129,8 @@
     loads = [
         pltpu.make_async_copy(src, dst, load_sem.at[n])
         for n, (src, dst) in enumerate(
-            ((sgate_in, sgate), (sup_in, sup), (sdown_in, sdown),
-             (gate_in.at[0], gate), (up_in.at[0], up), (down_in.at[0], down))
+            ((gate_in.at[0], gate), (up_in.at[0], up), (down_in.at[0], down),
+             (sgate_in, sgate), (sup_in, sup), (sdown_in, sdown))
         )
     ]
     for load in loads:
@@ -236,59 +236,89 @@
     def part_all(origin):
         return pl.ds(pl.multiple_of(origin * rows, 16), rows)
 
-    for load in loads[:3]:
-        load.wait()
-
     def keep(cols, piece):
         shared[:, cols] = piece
 
-    feed(lambda: own[...], rows, sgate, sup, sdown, keep)
-    for load in loads[3:]:
+    def pair_in(z, x):
+        for h in range(pieces):
+            arrived(device(z, x, 1 - core), h)
+
+    def onward_of(j):
+        return jnp.where(order[j] < level, level + 1, level - 1)
+
+    def fwd_copies(j, h):
+        origin = device(order[j], col, core)
+        return [
+            row_copy(rows_all, part(origin, h), origin, h, send, target)
+            for send, target in ((fwd_x_send.at[j, h], side), (fwd_twin_send.at[j, h], twin))
+        ]
+
+    def fwd(j):
+        for h in range(pieces):
+            fwd_piece(j, h)
+
+    def fwd_piece(j, h):
+        origin = device(order[j], col, core)
+        arrived(origin, h)
+        onward = onward_of(j)
+
+        @pl.when((onward >= 0) & (onward < zs))
+        def _():
+            row_copy(
+                rows_all, part(origin, h), origin, h, fwd_z_send.at[j, h],
+                device(onward, col, core),
+            ).start()
+
+        for copy in fwd_copies(j, h):
+            copy.start()
+
+    def across_in(j):
+        across = device(order[j], 1 - col, core)
+        for h in range(pieces):
+            arrived(across, h)
+            copy = row_copy(rows_all, part(across, h), across, h, fwd_twin_send.at[zs + j, h], twin)
+            copy.start()
+            sent.append(copy)
+
+    def own_chip(j):
+        pair_in(order[j], col)
+        chip(j, order[j], col)
+
+    def across_chip(j):
+        pair_in(order[j], 1 - col)
+        chip(zs + j, order[j], 1 - col)
+
+    inner = (level > 0) & (level < zs - 1)
+    outer = (level == 0) | (level == zs - 1)
+
+    for load in loads[:3]:
         load.wait()
     for step in range(1, count):
         remote(
             weights.at[me], weight_all.at[lax.rem(me + step, count)],
             w_send.at[step], w_recv.at[step], twin,
         ).wait_recv()
-
-    def pair_in(z, x):
-        for h in range(pieces):
-            arrived(device(z, x, 1 - core), h)
-
-    pair_in(level, col)
-    chip(0, level, col)
-    for j in range(1, zs + 1):
-        if j < zs:
-            origin_z = order[j]
-            origin = device(origin_z, col, core)
-            for h in range(pieces):
-                arrived(origin, h)
-                onward = jnp.where(origin_z < level, level + 1, level - 1)
-
-                @pl.when((onward >= 0) & (onward < zs))
-                def _():
-                    row_copy(
-                        rows_all, part(origin, h), origin, h, fwd_z_send.at[j, h],
-                        device(onward, col, core),
-                    ).start()
-
-                for send, target in ((fwd_x_send.at[j, h], side), (fwd_twin_send.at[j, h], twin)):
-                    copy = row_copy(rows_all, part(origin, h), origin, h, send, target)
-                    copy.start()
-                    sent.append(copy)
-        across = device(order[j - 1], 1 - col, core)
-        for h in range(pieces):
-            arrived(across, h)
-            copy = row_copy(
-                rows_all, part(across, h), across, h, fwd_twin_send.at[zs + j - 1, h], twin
-            )
-            copy.start()
-            sent.append(copy)
-        if j < zs:
-            pair_in(order[j], col)
-            chip(j, order[j], col)
-        pair_in(order[j - 1], 1 - col)
-        chip(zs + j - 1, order[j - 1], 1 - col)
+    own_chip(0)
+    for h in range(pieces):
+        fwd_piece(1, h)
+        pl.when(inner)(functools.partial(fwd_piece, 2, h))
+        if h == 0:
+            for load in loads[3:]:
+                load.wait()
+            feed(lambda: own[...], rows, sgate, sup, sdown, keep)
+    across_in(0)
+    own_chip(1)
+    across_chip(0)
+    for h in range(pieces):
+        pl.when(inner)(functools.partial(fwd_piece, 3, h))
+        pl.when(outer)(functools.partial(fwd_piece, 2, h))
+    across_in(1)
+    own_chip(2)
+    across_chip(1)
+    pl.when(outer)(functools.partial(fwd, 3))
+    across_in(2)
+    own_chip(3)
+    across_chip(2)
 
     def twin_in(label):
         remote(
@@ -320,7 +350,7 @@
 
         return store
 
-    for j in reversed(range(zs)):
+    def side_out(j):
         twin_in(zs + j)
         origin = device(order[j], 1 - col, core)
         for h in range(pieces):
@@ -330,6 +360,12 @@
                 side_send.at[j, h], side_recv.at[j, h], side,
             )
 
+    side_out(2)
+    across_in(3)
+    across_chip(3)
+    for j in (3, 1, 0):
+        side_out(j)
+
     def side_in(j, h):
         view = from_side.at[j, pl.ds(h * span, span)]
         remote(view, view, side_send.at[j, h], side_recv.at[j, h], side).wait_recv()
@@ -338,7 +374,7 @@
         view = from_far.at[slot, pl.ds(h * span, span)]
         remote(view, view, far_send.at[0, h], far_recv.at[slot, h], side).wait_recv()
 
-    for j in reversed(range(1, zs)):
+    for j in (2, 3, 1):
         twin_in(j)
         goal = order[j]
         origin = device(goal, col, core)
@@ -408,7 +444,9 @@
             row_copy(own, piece, me, h, own_z_send.at[1, h], twin).wait_send()
 
         for j in range(1, zs):
-            onward = jnp.where(order[j] < level, level + 1, level - 1)
+            for copy in fwd_copies(j, h):
+                copy.wait_send()
+            onward = onward_of(j)
 
             @pl.when((onward >= 0) & (onward < zs))
             def _():

time: 114 us -> 103 us (0.904)
  Pallas kernels: 108 us -> 95.9 us
    pallas_call x1, Pallas kernels: 97.1 us -> 85.6 us  [expert_stage(): pl.pallas_call(functools.partial(expert_kernel, grid_shape, pieces), out_...]
where the time goes in v4:
time: 103 us; the launch traced here: 102 us
  Pallas kernels  95.9 us (93%)
  local copies, waits for them, and re-layouts  3.36 us (3%)
  other arithmetic  2.4 us (2%)
    pallas_call x1, Pallas kernels, expert_stage(): pl.pallas_call(functools.partial(expert_kernel, grid_shape, pieces), out_...  85.6 us
    pallas_call x1, Pallas kernels, mixer_stage(): pl.pallas_call(mixer_kernel, grid=(channels // block,), out_shape=(jax.Sh...  10.4 us

profile of v4, /device:TPU:0, one launch (start us, length us, event | category | flops | bytes accessed | tf_op | source)
XLA Modules:
  0.0 102.4 jit_solution(9142354470045654508)
XLA Ops:
  0.6 0.7 exp.6
  1.3 0.7 select_reduce_fusion
  2.0 0.6 pad.4
  2.6 1.0 cosine_multiply_fusion
  3.6 0.1 stack.15
  3.7 0.1 stack.17
  3.8 0.1 stack.18
  3.9 0.1 stack.16
  4.0 0.7 pad_maximum_fusion.params
  4.7 10.4 %shard_map.203 = (f32[2,96,4096]{2,1,0:T(8,128)}, bf16[96,2048]{1,0:T(8,128)(2,1)}, bf16[96,2048]{1,0:T(8,128)(2,1)}) custom-call(bf16[96,2048]{1,0:T(8,128)(2,1)} %tokens.1, f32[2,96,4096]{2,1,0:T(8,128)} %prior.1, f32[1,2048]{1,0:T(1,128)} %bitcast.11, bf16[2048,1024]{1,0:T(8,128)(2,1)} %in_weight.1, f32[4,4096]{1,0:T(4,128)} %pad_maximum_fusion.params, ...), custom_call_target="tpu_custom_call" | custom-call | tf_op jit(solution)/shard_map/pallas_call | solution.py:617
  15.0 85.6 %shard_map.204 = bf16[96,2048]{1,0:T(8,128)(2,1)} custom-call(bf16[96,2048]{1,0:T(8,128)(2,1)} %get-tuple-element.5.own, bf16[96,2048]{1,0:T(8,128)(2,1)} %get-tuple-element.6.middle, f32[16,1,128]{2,1,0:T(1,128)} %bitcast.10, bf16[1,2048,512]{2,1,0:T(8,128)(2,1)} %gate_in.1, bf16[1,2048,512]{2,1,0:T(8,128)(2,1)} %up_in.1, bf16[1,512,2048]{2,1,0:T(8,128)(2,1)} %down_in.1, ...), custom_call_target="tpu_custom_call" | custom-call | tf_op jit(solution)/shard_map/pallas_call | solution.py:473
  100.6 1.8 %copy.25 = bf16[96,2048]{1,0:T(8,128)(2,1)} copy(bf16[96,2048]{1,0:T(8,128)(2,1)} %shard_map.204) | data formatting | bytes 786432

commit v5 on v4

--- a/solution.py
+++ b/solution.py
@@ -98,13 +98,14 @@
 
 
 def expert_kernel(
-    grid_shape, pieces,
+    grid_shape, cuts,
     own, middle, weights, gate_in, up_in, down_in, sgate_in, sup_in, sdown_in,
     out,
-    rows_all, back, from_twin, from_side, from_far, weight_all,
+    rows_all, back, from_twin, from_side, from_far, from_bent, weight_all,
     gate, up, down, sgate, sup, sdown, hidden, shared, total,
     load_sem, row_recv, own_z_send, fwd_z_send, fwd_x_send, fwd_twin_send,
     w_send, w_recv, twin_send, twin_recv, side_send, side_recv, far_send, far_recv,
+    bent_send, bent_far_send, bent_far_recv,
 ):
     zs, xs, cs = grid_shape
     count = zs * xs * cs
@@ -113,7 +114,9 @@
     col = lax.rem(me // cs, xs)
     level = me // (cs * xs)
     rows, width = own.shape
-    span = rows // pieces
+    pieces = len(cuts)
+    straight = range(pieces - 1)
+    bent = pieces - 1
     hid = gate.shape[1]
 
     def device(z, x, c):
@@ -124,7 +127,10 @@
     order = [looked_up([row[j] for row in near_first(zs)], level) for j in range(zs)]
 
     def part(base, h):
-        return pl.ds(pl.multiple_of(base * rows + h * span, 16), span)
+        return pl.ds(pl.multiple_of(base * rows + cuts[h][0], 16), cuts[h][1])
+
+    def local(h):
+        return pl.ds(cuts[h][0], cuts[h][1])
 
     loads = [
         pltpu.make_async_copy(src, dst, load_sem.at[n])
@@ -161,8 +167,8 @@
             src_ref.at[src_rows], rows_all.at[part(origin, h)], send, row_recv.at[origin, h], target
         )
 
-    for h in range(pieces):
-        piece = pl.ds(h * span, span)
+    for h in (bent, *straight):
+        piece = local(h)
 
         @pl.when(level > 0)
         def _():
@@ -182,13 +188,12 @@
         push(
             weights.at[other], weight_all.at[me], w_send.at[step], w_recv.at[count - step], other
         )
-    rows_all[part(me, 0), :] = own[pl.ds(0, span), :]
-    for h in range(1, pieces):
-        rows_all[part(me, h), :] = own[pl.ds(h * span, span), :]
+    for h in range(pieces):
+        rows_all[part(me, h), :] = own[local(h), :]
     weight_all[me] = weights[me]
 
     def arrived(origin, h):
-        row_copy(own, pl.ds(h * span, span), origin, h, own_z_send.at[0, h], twin).wait_recv()
+        row_copy(own, local(h), origin, h, own_z_send.at[0, h], twin).wait_recv()
 
     def feed(source, take, gate_w, up_w, down_w, finish):
         def first(n, carry):
@@ -250,12 +255,38 @@
         origin = device(order[j], col, core)
         return [
             row_copy(rows_all, part(origin, h), origin, h, send, target)
-            for send, target in ((fwd_x_send.at[j, h], side), (fwd_twin_send.at[j, h], twin))
-        ]
+            for send, target in ((fwd_twin_send.at[j, h], twin), (fwd_x_send.at[j, h], side))
+        ][: 1 if h == bent else 2]
 
     def fwd(j):
-        for h in range(pieces):
+        for h in (bent, *straight):
             fwd_piece(j, h)
+        bent_across(j)
+
+    def bent_copies(j):
+        origin = device(order[j], 1 - col, core)
+
+        def one(send, target):
+            return row_copy(rows_all, part(origin, bent), origin, bent, send, target)
+
+        if j == 0:
+            moves = [
+                (level > 0, one(bent_send.at[0], device(level - 1, col, core))),
+                (level < zs - 1, one(bent_send.at[zs], device(level + 1, col, core))),
+            ]
+        else:
+            onward = onward_of(j)
+            moves = [
+                ((onward >= 0) & (onward < zs), one(bent_send.at[j], device(onward, col, core)))
+            ]
+        return moves, one(fwd_twin_send.at[zs + j, bent], twin)
+
+    def bent_across(j):
+        arrived(device(order[j], 1 - col, core), bent)
+        moves, to_twin = bent_copies(j)
+        for allowed, copy in moves:
+            pl.when(allowed)(copy.start)
+        to_twin.start()
 
     def fwd_piece(j, h):
         origin = device(order[j], col, core)
@@ -274,7 +305,7 @@
 
     def across_in(j):
         across = device(order[j], 1 - col, core)
-        for h in range(pieces):
+        for h in straight:
             arrived(across, h)
             copy = row_copy(rows_all, part(across, h), across, h, fwd_twin_send.at[zs + j, h], twin)
             copy.start()
@@ -299,19 +330,21 @@
             w_send.at[step], w_recv.at[step], twin,
         ).wait_recv()
     own_chip(0)
-    for h in range(pieces):
+    bent_across(0)
+    for h in (bent, *straight):
         fwd_piece(1, h)
         pl.when(inner)(functools.partial(fwd_piece, 2, h))
         if h == 0:
             for load in loads[3:]:
                 load.wait()
             feed(lambda: own[...], rows, sgate, sup, sdown, keep)
+    bent_across(1)
+    pl.when(inner)(functools.partial(bent_across, 2))
     across_in(0)
     own_chip(1)
     across_chip(0)
-    for h in range(pieces):
-        pl.when(inner)(functools.partial(fwd_piece, 3, h))
-        pl.when(outer)(functools.partial(fwd_piece, 2, h))
+    pl.when(inner)(functools.partial(fwd, 3))
+    pl.when(outer)(functools.partial(fwd, 2))
     across_in(1)
     own_chip(2)
     across_chip(1)
@@ -325,7 +358,7 @@
             from_twin.at[label], from_twin.at[label], twin_send.at[label], twin_recv.at[label], twin
         ).wait_recv()
 
-    def added(first, others, store):
+    def added(h, first, others, store):
         def strip(n, carry):
             at = pl.multiple_of(n * 16, 16)
             value = first(at).astype(jnp.float32)
@@ -334,17 +367,17 @@
             store(at, value)
             return carry
 
-        lax.fori_loop(0, span // 16, strip, 0)
+        lax.fori_loop(0, cuts[h][1] // 16, strip, 0)
 
     def back_at(origin, h):
-        return lambda at: back[pl.ds(pl.multiple_of(origin * rows + h * span + at, 16), 16), :]
+        return lambda at: back[pl.ds(pl.multiple_of(origin * rows + cuts[h][0] + at, 16), 16), :]
 
     def slot_at(ref, slot, h):
-        return lambda at: ref[slot, pl.ds(pl.multiple_of(h * span + at, 16), 16), :]
+        return lambda at: ref[slot, pl.ds(pl.multiple_of(cuts[h][0] + at, 16), 16), :]
 
     def to_back(origin, h):
         def store(at, value):
-            back[pl.ds(pl.multiple_of(origin * rows + h * span + at, 16), 16), :] = value.astype(
+            back[pl.ds(pl.multiple_of(origin * rows + cuts[h][0] + at, 16), 16), :] = value.astype(
                 jnp.bfloat16
             )
 
@@ -353,12 +386,66 @@
     def side_out(j):
         twin_in(zs + j)
         origin = device(order[j], 1 - col, core)
-        for h in range(pieces):
-            added(back_at(origin, h), [slot_at(from_twin, zs + j, h)], to_back(origin, h))
-            push(
-                back.at[part(origin, h)], from_side.at[j, pl.ds(h * span, span)],
-                side_send.at[j, h], side_recv.at[j, h], side,
-            )
+        for h in straight:
+            added(h, back_at(origin, h), [slot_at(from_twin, zs + j, h)], to_back(origin, h))
+            side_push(j, h)
+
+    def side_push(j, h):
+        origin = device(order[j], 1 - col, core)
+        push(
+            back.at[part(origin, h)], from_side.at[j, local(h)],
+            side_send.at[j, h], side_recv.at[j, h], side,
+        )
+
+    def side_in(j, h):
+        view = from_side.at[j, local(h)]
+        remote(view, view, side_send.at[j, h], side_recv.at[j, h], side).wait_recv()
+
+    def far_in(ref, recv, slot, h):
+        view = ref.at[slot, local(h)]
+        remote(view, view, far_send.at[0, h], recv.at[slot, h], side).wait_recv()
+
+    def chain(j, lane, ref, send, recv, label, h, extra):
+        goal = order[j]
+        origin = device(goal, lane, core)
+        nearer = jnp.where(goal < level, level - 1, level + 1)
+        behind = jnp.where(goal < level, level + 1, level - 1)
+        slot = jnp.where((nearer == goal) & (goal > level), zs, goal)
+        terms = [slot_at(from_twin, label, h)] + extra
+
+        @pl.when((behind >= 0) & (behind < zs))
+        def _():
+            far_in(ref, recv, goal, h)
+            added(h, back_at(origin, h), terms + [slot_at(ref, goal, h)], to_back(origin, h))
+
+        @pl.when((behind < 0) | (behind >= zs))
+        def _():
+            added(h, back_at(origin, h), terms, to_back(origin, h))
+
+        push(
+            back.at[part(origin, h)], ref.at[slot, local(h)],
+            send.at[j, h], recv.at[slot, h], device(nearer, col, core),
+        )
+
+    def gather_far(h, ref, recv):
+        @pl.when(level > 0)
+        def _():
+            far_in(ref, recv, zs, h)
+            added(h, total_at(h), [slot_at(ref, zs, h)], to_total(h))
+
+        @pl.when(level < zs - 1)
+        def _():
+            far_in(ref, recv, level, h)
+            added(h, total_at(h), [slot_at(ref, level, h)], to_total(h))
+
+    def to_total(h):
+        def store(at, value):
+            total[pl.ds(pl.multiple_of(cuts[h][0] + at, 16), 16), :] = value
+
+        return store
+
+    def total_at(h):
+        return lambda at: total[pl.ds(pl.multiple_of(cuts[h][0] + at, 16), 16), :]
 
     side_out(2)
     across_in(3)
@@ -366,74 +453,44 @@
     for j in (3, 1, 0):
         side_out(j)
 
-    def side_in(j, h):
-        view = from_side.at[j, pl.ds(h * span, span)]
-        remote(view, view, side_send.at[j, h], side_recv.at[j, h], side).wait_recv()
-
-    def far_in(slot, h):
-        view = from_far.at[slot, pl.ds(h * span, span)]
-        remote(view, view, far_send.at[0, h], far_recv.at[slot, h], side).wait_recv()
+    for j in (2, 3, 1):
+        chain(j, 1 - col, from_bent, bent_far_send, bent_far_recv, zs + j, bent, [])
+    origin = device(level, 1 - col, core)
+    added(bent, back_at(origin, bent), [slot_at(from_twin, zs, bent)], to_total(bent))
+    gather_far(bent, from_bent, bent_far_recv)
+    added(bent, total_at(bent), [], to_back(origin, bent))
+    side_push(0, bent)
 
     for j in (2, 3, 1):
         twin_in(j)
-        goal = order[j]
-        origin = device(goal, col, core)
-        nearer = jnp.where(goal < level, level - 1, level + 1)
-        behind = jnp.where(goal < level, level + 1, level - 1)
-        slot = jnp.where((nearer == goal) & (goal > level), zs, goal)
-        for h in range(pieces):
+        chain(j, col, from_far, far_send, far_recv, j, bent, [])
+        for h in straight:
             side_in(j, h)
-            terms = [slot_at(from_twin, j, h), slot_at(from_side, j, h)]
-
-            @pl.when((behind >= 0) & (behind < zs))
-            def _():
-                far_in(goal, h)
-                added(
-                    back_at(origin, h), terms + [slot_at(from_far, goal, h)], to_back(origin, h)
-                )
-
-            @pl.when((behind < 0) | (behind >= zs))
-            def _():
-                added(back_at(origin, h), terms, to_back(origin, h))
-
-            push(
-                back.at[part(origin, h)], from_far.at[slot, pl.ds(h * span, span)],
-                far_send.at[j, h], far_recv.at[slot, h], device(nearer, col, core),
-            )
+            chain(j, col, from_far, far_send, far_recv, j, h, [slot_at(from_side, j, h)])
     twin_in(0)
     for h in range(pieces):
         side_in(0, h)
-
-        def to_total(at, value):
-            total[pl.ds(pl.multiple_of(h * span + at, 16), 16), :] = value
-
-        def total_at(at):
-            return total[pl.ds(pl.multiple_of(h * span + at, 16), 16), :]
-
-        added(back_at(me, h), [slot_at(from_twin, 0, h), slot_at(from_side, 0, h)], to_total)
-
-        @pl.when(level > 0)
-        def _():
-            far_in(zs, h)
-            added(total_at, [slot_at(from_far, zs, h)], to_total)
-
-        @pl.when(level < zs - 1)
-        def _():
-            far_in(level, h)
-            added(total_at, [slot_at(from_far, level, h)], to_total)
+        terms = [slot_at(from_twin, 0, h), slot_at(from_side, 0, h)]
+        added(h, back_at(me, h), terms, to_total(h))
+        gather_far(h, from_far, far_recv)
 
         def plain(ref):
-            return lambda at: ref[pl.ds(pl.multiple_of(h * span + at, 16), 16), :]
+            return lambda at: ref[pl.ds(pl.multiple_of(cuts[h][0] + at, 16), 16), :]
 
         def to_out(at, value):
-            out[pl.ds(pl.multiple_of(h * span + at, 16), 16), :] = value.astype(jnp.bfloat16)
-
-        added(plain(middle), [total_at, plain(shared)], to_out)
-
+            out[pl.ds(pl.multiple_of(cuts[h][0] + at, 16), 16), :] = value.astype(jnp.bfloat16)
+
+        added(h, plain(middle), [total_at(h), plain(shared)], to_out)
+
+    for j in range(zs):
+        moves, to_twin = bent_copies(j)
+        for allowed, copy in moves:
+            pl.when(allowed)(copy.wait_send)
+        to_twin.wait_send()
     for copy in sent:
         copy.wait_send()
     for h in range(pieces):
-        piece = pl.ds(h * span, span)
+        piece = local(h)
 
         @pl.when(level > 0)
         def _():
@@ -462,7 +519,10 @@
     zs = grid_shape[0]
     rows, width = second_normed.shape
     hid = expert_gate.shape[2]
-    pieces = 2 if rows % 32 == 0 else 1
+    small = max(16, rows // 6 // 16 * 16)
+    first = (rows - small) // 32 * 16 + (rows - small) // 16 % 2 * 16
+    cuts = ((0, first), (first, rows - small - first), (rows - small, small))
+    pieces = len(cuts)
     chosen = routes[None, :, :] == jnp.arange(experts, dtype=jnp.int32)[:, None, None]
     weights = jnp.sum(jnp.where(chosen, route_weights[None], 0.0), axis=2)
     weights = jnp.pad(weights, ((0, 0), (0, 128 - rows)))[:, None, :]
@@ -471,7 +531,7 @@
     dma = pltpu.SemaphoreType.DMA
     half = jnp.bfloat16
     return pl.pallas_call(
-        functools.partial(expert_kernel, grid_shape, pieces),
+        functools.partial(expert_kernel, grid_shape, cuts),
         out_shape=jax.ShapeDtypeStruct((rows, width), half),
         in_specs=[vmem] * 3 + [hbm] * 6,
         out_specs=vmem,
@@ -480,6 +540,7 @@
             pltpu.VMEM((experts * rows, width), half),
             pltpu.VMEM((2 * zs, rows, width), half),
             pltpu.VMEM((zs, rows, width), half),
+            pltpu.VMEM((zs + 1, rows, width), half),
             pltpu.VMEM((zs + 1, rows, width), half),
             pltpu.VMEM((experts, 1, 128), jnp.float32),
             pltpu.VMEM((width, hid), half),
@@ -503,6 +564,9 @@
             dma((2 * zs,)),
             dma((zs, pieces)),
             dma((zs, pieces)),
+            dma((zs, pieces)),
+            dma((zs + 1, pieces)),
+            dma((zs + 1,)),
             dma((zs, pieces)),
             dma((zs + 1, pieces)),
         ],

time: 103 us -> 115 us (1.12)
  Pallas kernels: 95.9 us -> 108 us
    pallas_call x1, Pallas kernels: 85.6 us -> 98 us  [expert_stage(): pl.pallas_call(functools.partial(expert_kernel, grid_shape, cuts), out_sh...]
where the time goes in v5:
time: 115 us
  Pallas kernels  108 us (94%)
  local copies, waits for them, and re-layouts  3.36 us (3%)
  other arithmetic  2.4 us (2%)
    pallas_call x1, Pallas kernels, expert_stage(): pl.pallas_call(functools.partial(expert_kernel, grid_shape, cuts), out_sh...  98 us
    pallas_call x1, Pallas kernels, mixer_stage(): pl.pallas_call(mixer_kernel, grid=(channels // block,), out_shape=(jax.Sh...  10.4 us

profile of v5, /device:TPU:0, one launch (start us, length us, event | category | flops | bytes accessed | tf_op | source)
XLA Modules:
  0.0 114.8 jit_solution(1028146165139105060)
XLA Ops:
  0.6 0.7 exp.6
  1.3 0.7 select_reduce_fusion
  2.0 0.6 pad.4
  2.6 1.0 cosine_multiply_fusion
  3.6 0.1 stack.15
  3.7 0.1 stack.17
  3.8 0.1 stack.18
  3.9 0.1 stack.16
  4.0 0.7 pad_maximum_fusion.params
  4.7 10.4 %shard_map.203 = (f32[2,96,4096]{2,1,0:T(8,128)}, bf16[96,2048]{1,0:T(8,128)(2,1)}, bf16[96,2048]{1,0:T(8,128)(2,1)}) custom-call(bf16[96,2048]{1,0:T(8,128)(2,1)} %tokens.1, f32[2,96,4096]{2,1,0:T(8,128)} %prior.1, f32[1,2048]{1,0:T(1,128)} %bitcast.11, bf16[2048,1024]{1,0:T(8,128)(2,1)} %in_weight.1, f32[4,4096]{1,0:T(4,128)} %pad_maximum_fusion.params, ...), custom_call_target="tpu_custom_call" | custom-call | tf_op jit(solution)/shard_map/pallas_call | solution.py:681
  15.0 98.0 %shard_map.204 = bf16[96,2048]{1,0:T(8,128)(2,1)} custom-call(bf16[96,2048]{1,0:T(8,128)(2,1)} %get-tuple-element.5.own, bf16[96,2048]{1,0:T(8,128)(2,1)} %get-tuple-element.6.middle, f32[16,1,128]{2,1,0:T(1,128)} %bitcast.10, bf16[1,2048,512]{2,1,0:T(8,128)(2,1)} %gate_in.1, bf16[1,2048,512]{2,1,0:T(8,128)(2,1)} %up_in.1, bf16[1,512,2048]{2,1,0:T(8,128)(2,1)} %down_in.1, ...), custom_call_target="tpu_custom_call" | custom-call | tf_op jit(solution)/shard_map/pallas_call | solution.py:533
  113.0 1.8 %copy.25 = bf16[96,2048]{1,0:T(8,128)(2,1)} copy(bf16[96,2048]{1,0:T(8,128)(2,1)} %shard_map.204) | data formatting | bytes 786432

commit v6 on v4

--- a/solution.py
+++ b/solution.py
@@ -462,7 +462,7 @@
     zs = grid_shape[0]
     rows, width = second_normed.shape
     hid = expert_gate.shape[2]
-    pieces = 2 if rows % 32 == 0 else 1
+    pieces = 3 if rows % 48 == 0 else 1
     chosen = routes[None, :, :] == jnp.arange(experts, dtype=jnp.int32)[:, None, None]
     weights = jnp.sum(jnp.where(chosen, route_weights[None], 0.0), axis=2)
     weights = jnp.pad(weights, ((0, 0), (0, 128 - rows)))[:, None, :]

time: 103 us -> 102 us (level)
  no operation moved by 1% of the time
where the time goes in v6:
time: 102 us
  Pallas kernels  95.5 us (94%)
  local copies, waits for them, and re-layouts  3.36 us (3%)
  other arithmetic  2.4 us (2%)
    pallas_call x1, Pallas kernels, expert_stage(): pl.pallas_call(functools.partial(expert_kernel, grid_shape, pieces), out_...  85.1 us
    pallas_call x1, Pallas kernels, mixer_stage(): pl.pallas_call(mixer_kernel, grid=(channels // block,), out_shape=(jax.Sh...  10.4 us

profile of v6, /device:TPU:0, one launch (start us, length us, event | category | flops | bytes accessed | tf_op | source)
XLA Modules:
  0.0 101.9 jit_solution(5469589380774440581)
XLA Ops:
  0.6 0.7 exp.6
  1.3 0.7 select_reduce_fusion
  2.0 0.6 pad.4
  2.6 1.0 cosine_multiply_fusion
  3.6 0.1 stack.15
  3.7 0.1 stack.17
  3.8 0.1 stack.18
  3.9 0.1 stack.16
  4.0 0.7 pad_maximum_fusion.params
  4.7 10.4 %shard_map.203 = (f32[2,96,4096]{2,1,0:T(8,128)}, bf16[96,2048]{1,0:T(8,128)(2,1)}, bf16[96,2048]{1,0:T(8,128)(2,1)}) custom-call(bf16[96,2048]{1,0:T(8,128)(2,1)} %tokens.1, f32[2,96,4096]{2,1,0:T(8,128)} %prior.1, f32[1,2048]{1,0:T(1,128)} %bitcast.11, bf16[2048,1024]{1,0:T(8,128)(2,1)} %in_weight.1, f32[4,4096]{1,0:T(4,128)} %pad_maximum_fusion.params, ...), custom_call_target="tpu_custom_call" | custom-call | tf_op jit(solution)/shard_map/pallas_call | solution.py:617
  15.0 85.1 %shard_map.204 = bf16[96,2048]{1,0:T(8,128)(2,1)} custom-call(bf16[96,2048]{1,0:T(8,128)(2,1)} %get-tuple-element.5.own, bf16[96,2048]{1,0:T(8,128)(2,1)} %get-tuple-element.6.middle, f32[16,1,128]{2,1,0:T(1,128)} %bitcast.10, bf16[1,2048,512]{2,1,0:T(8,128)(2,1)} %gate_in.1, bf16[1,2048,512]{2,1,0:T(8,128)(2,1)} %up_in.1, bf16[1,512,2048]{2,1,0:T(8,128)(2,1)} %down_in.1, ...), custom_call_target="tpu_custom_call" | custom-call | tf_op jit(solution)/shard_map/pallas_call | solution.py:473
  100.2 1.8 %copy.25 = bf16[96,2048]{1,0:T(8,128)(2,1)} copy(bf16[96,2048]{1,0:T(8,128)(2,1)} %shard_map.204) | data formatting | bytes 786432
